TPU v7x, 512 devices: a 8x2x16 block of a 8x8x16 slice. The times are simulated.
512 devices in a mesh: grp: 2 (over y), sp: 32 (over z, core), tp: 8 (over x).
Axes of the slice: x: 8, y: 2, z: 16, core: 2. Of those that a mesh axis runs over, the one named last changes fastest.
The devices are a block of a 8x8x16 slice.
Arguments:
- residual: bfloat16 [16384, 2048], P(('grp', 'sp')), parts along dimension 0, may hold values from -34 to 34
- queries: bfloat16 [16384, 1024], P(('grp', 'sp'), 'tp'), parts along dimension 0, may hold values from -400 to 400
- keys: bfloat16 [16384, 512], P(('grp', 'sp'), 'tp'), parts along dimension 0, may hold values from -8 to 8
- values: bfloat16 [16384, 512], P(('grp', 'sp'), 'tp'), parts along dimension 0, may hold values from -6 to 6
- segments: int32 [16384], P(('grp', 'sp')), parts along dimension 0, may hold values from 0 to 16, never falling along the last dimension, each value on 1 to 768 neighbouring positions
- routes: int32 [16384, 2], P(('grp', 'sp')), parts along dimension 0, may hold values from 0 to 31, all different within a row; in each aligned block of 256 rows (0 to 255, 256 to 511, ...) at most 32 rows name the same one
- route_weight: float32 [16384, 2], P(('grp', 'sp')), parts along dimension 0, may hold values from 0.3 to 3
- sinks: float32 [16], P('tp'), may hold values from 1 to 6
- out_weight: bfloat16 [1024, 2048], P('tp'), may hold values from -1 to 1
- norm_gain: float32 [2048], replicated, may hold values from 0.1 to 1.9
- expert_gate: bfloat16 [32, 2048, 1024], P('sp', None, 'tp'), may hold values from -0.125 to 0.125
- expert_up: bfloat16 [32, 2048, 1024], P('sp', None, 'tp'), may hold values from -0.125 to 0.125
- expert_down: bfloat16 [32, 1024, 2048], P('sp', None, 'tp'), may hold values from -0.1875 to 0.1875
- shared_gate: bfloat16 [2048, 1024], P(None, 'tp'), may hold values from -0.125 to 0.125
- shared_up: bfloat16 [2048, 1024], P(None, 'tp'), may hold values from -0.125 to 0.125
- shared_down: bfloat16 [1024, 2048], P(None, 'tp'), may hold values from -0.1875 to 0.1875
Outputs:
- mixed: bfloat16 [16384, 2048], P(('grp', 'sp'), 'tp'), parts along dimension 0
There are 2 independent parts, one for each index of `grp`. A program takes and returns all parts, laid end to end along the dimension named above; an argument that names none is the same for every part. Nothing has to cross between parts.
Inputs may be any that keep to these rules, and one draw needn't show every extreme that they name: `routes`: each row names 2 different experts. In the rows of one device no expert is named by more than 32 rows, and in some device's rows an expert is named by exactly 32. `segments`: document numbers never fall along the positions; every document spans 1 to 768 positions and one spans exactly 768.
All inputs are finite; a program needn't handle non-finite values.
Results may differ from a plain program's by a relative error of at most 0.0065.
Values may be sent and summed in bfloat16 or wider, within the bound.
A program may use at most 64 MiB of HBM per device.

v0:
```python
import jax
import jax.numpy as jnp
from jax import lax
from jax.sharding import Mesh
from jax.sharding import PartitionSpec as P

HEAD_DIM = 64
WINDOW = 128
SP = ("sp_0", "sp_1")
GRP_SP = ("grp", "sp_0", "sp_1")


epsilon = 1e-06


def passed_along(value, axis, steps):
    count = lax.axis_size(axis)
    leading, last = (max(0, -steps), min(count, count - steps))
    return lax.ppermute(value, axis, [(source, source + steps) for source in range(leading, last)])


def split_up(array, dim, size):
    shape = array.shape
    blocks = array.reshape(*shape[:dim], size, shape[dim] // size, *shape[dim + 1 :])
    return jnp.moveaxis(blocks, dim, 0)


def sent_and_summed(array, axis, dim):
    size = lax.axis_size(axis)
    blocks = lax.all_to_all(split_up(array, dim, size), axis, 0, 0, tiled=True)
    return jnp.sum(blocks.astype(jnp.float32), axis=0)


def sent_to_all(array, axis):
    size = lax.axis_size(axis)
    return lax.all_to_all(
        jnp.broadcast_to(array[None], (size, *array.shape)), axis, 0, 0, tiled=True
    )


def in_order(blocks, dim):
    blocks = jnp.moveaxis(blocks, 0, dim)
    shape = blocks.shape
    return blocks.reshape(*shape[:dim], shape[dim] * shape[dim + 1], *shape[dim + 2 :])


def collect(array, axis, dim):
    blocks = sent_to_all(array, axis)
    return in_order(blocks, dim)


def moved_by_axis(blocks, axes, order):
    shape = [lax.axis_size(a) for a in axes]
    blocks = blocks.reshape(*shape, *blocks.shape[1:])
    for k in order:
        blocks = lax.all_to_all(blocks, axes[k], split_axis=k, concat_axis=k, tiled=True)
    return blocks.reshape(-1, *blocks.shape[len(axes) :])


def two_step_exchange(array, groups, order, split_dim, concat_dim):
    size = lax.axis_size(groups[0]) * lax.axis_size(groups[1])
    blocks = split_up(array, split_dim, size)
    return in_order(moved_by_axis(blocks, groups, order), concat_dim)


def sent_together(arrays, axis, dim, along):
    ends, at = ([], 0)
    for a in arrays[:-1]:
        at += a.shape[along]
        ends.append(at)
    both = jnp.concatenate(arrays, axis=along)
    return tuple(jnp.split(lax.all_gather(both, axis, axis=dim, tiled=True), ends, axis=along))


def banded(prev_rows, own_rows, window_len):
    blocks = own_rows.shape[0] // window_len
    joined = jnp.concatenate([prev_rows, own_rows], axis=0)
    shaped = joined.reshape((blocks + 1, window_len) + own_rows.shape[1:])
    return jnp.concatenate([shaped[:-1], shaped[1:]], axis=1)


def shards(
    residual,
    queries,
    keys,
    values,
    segments,
    routes,
    route_weight,
    sinks,
    out_weight,
    norm_gain,
    expert_gate,
    expert_up,
    expert_down,
    shared_gate,
    shared_up,
    shared_down,
):
    rows_here = residual.shape[0]
    model_width = residual.shape[1]
    tp_count = lax.axis_size("tp")
    tp_index = lax.axis_index("tp")
    head_local = queries.shape[1] // HEAD_DIM
    kv_local = keys.shape[1] // HEAD_DIM
    group_size = head_local // kv_local
    window_len = WINDOW
    blocks = rows_here // window_len
    own_marks = (segments % 256 + 1).astype(jnp.bfloat16)
    prev_keys, prev_values, prev_marks = passed_along(
        (
            keys[rows_here - window_len :],
            values[rows_here - window_len :],
            own_marks[rows_here - window_len :],
        ),
        SP,
        1,
    )
    key_band = banded(prev_keys, keys, window_len).reshape(
        blocks, 2 * window_len, kv_local, HEAD_DIM
    )
    value_band = banded(prev_values, values, window_len).reshape(
        blocks, 2 * window_len, kv_local, HEAD_DIM
    )
    mark_band = banded(prev_marks, own_marks, window_len).astype(jnp.float32)
    query_marks = own_marks.reshape(blocks, window_len).astype(jnp.float32)
    query_blocks = queries.reshape(blocks, window_len, kv_local, group_size, HEAD_DIM)
    scores = jnp.einsum(
        "nqhgd,nkhd->nhgqk", query_blocks, key_band, preferred_element_type=jnp.float32
    ) * HEAD_DIM ** (-0.5)
    offsets = jnp.arange(window_len)[:, None] + window_len - jnp.arange(2 * window_len)[None, :]
    allowed = (
        (offsets >= 0) & (offsets < window_len) & (query_marks[:, :, None] == mark_band[:, None, :])
    )
    sink_logits = sinks.reshape(kv_local, group_size)[None, :, :, None]
    masked = jnp.where(allowed[:, None, None], scores, -jnp.inf)
    top_score = jnp.maximum(jnp.max(masked, axis=-1), sink_logits)
    exp_terms = jnp.where(allowed[:, None, None], jnp.exp(scores - top_score[..., None]), 0.0)
    denominator = jnp.sum(exp_terms, axis=-1) + jnp.exp(sink_logits - top_score)
    probabilities = (exp_terms / denominator[..., None]).astype(jnp.bfloat16)
    attended = jnp.einsum(
        "nhgqk,nkhd->nqhgd", probabilities, value_band, preferred_element_type=jnp.float32
    )
    attended = attended.astype(jnp.bfloat16).reshape(rows_here, head_local * HEAD_DIM)
    partial_value = jnp.dot(attended, out_weight, preferred_element_type=jnp.float32)
    col_width = model_width // tp_count
    col_start = tp_index * col_width
    share_sum = sent_and_summed(partial_value.astype(jnp.bfloat16), "tp", 1)
    residual_cols = lax.dynamic_slice_in_dim(residual, col_start, col_width, 1)
    updated_cols = (residual_cols.astype(jnp.float32) + share_sum).astype(jnp.bfloat16)
    cols_f32 = updated_cols.astype(jnp.float32)
    squares = lax.psum(jnp.sum(cols_f32 * cols_f32, axis=-1), "tp")
    inv_rms = lax.rsqrt(squares / model_width + epsilon)
    gain_cols = lax.dynamic_slice_in_dim(norm_gain, col_start, col_width, 0)
    normed_cols = (cols_f32 * inv_rms[:, None] * gain_cols).astype(jnp.bfloat16)
    normed = collect(normed_cols, "tp", 1)
    shared_pre = jnp.dot(normed, shared_gate, preferred_element_type=jnp.float32)
    shared_lin = jnp.dot(normed, shared_up, preferred_element_type=jnp.float32)
    shared_act = (jax.nn.silu(shared_pre) * shared_lin).astype(jnp.bfloat16)
    top_count = routes.shape[1]
    experts = lax.axis_size(SP)
    capacity = 2 * rows_here * top_count // experts
    flat_ids = routes.reshape(-1)
    one_hot = (flat_ids[:, None] == jnp.arange(experts, dtype=jnp.int32)[None, :]).astype(jnp.int32)
    rank_in = jnp.cumsum(one_hot, axis=0) - one_hot
    slot_dest = flat_ids * capacity + jnp.sum(rank_in * one_hot, axis=1)
    token_of = jnp.arange(rows_here * top_count, dtype=jnp.int32) // top_count
    slot_token = jnp.full((experts * capacity,), -1, jnp.int32).at[slot_dest].set(token_of)
    filled = slot_token >= 0
    safe_token = jnp.where(filled, slot_token, 0)
    outgoing = jnp.where(filled[:, None], normed_cols[safe_token], jnp.zeros((), jnp.bfloat16))
    pieces = two_step_exchange(
        outgoing.reshape(experts, capacity, col_width), ("sp_0", "sp_1"), (1, 0), 0, 0
    )
    arrived = lax.all_gather(pieces, "tp", axis=2, tiled=True)
    expert_rows = arrived.reshape(-1, model_width)
    gate_pre = jnp.dot(expert_rows, expert_gate[0], preferred_element_type=jnp.float32)
    up_lin = jnp.dot(expert_rows, expert_up[0], preferred_element_type=jnp.float32)
    expert_act = (jax.nn.silu(gate_pre) * up_lin).astype(jnp.bfloat16)
    gathered_expert, gathered_shared = sent_together((expert_act, shared_act), "tp", 1, 0)
    expert_out = jnp.dot(
        gathered_expert, expert_down[0], preferred_element_type=jnp.float32
    ).astype(jnp.bfloat16)
    returned = lax.all_to_all(
        expert_out.reshape(experts, capacity, col_width),
        SP,
        split_axis=0,
        concat_axis=0,
        tiled=True,
    )
    returned = returned.reshape(experts * capacity, col_width)
    picked = returned[slot_dest].astype(jnp.float32).reshape(rows_here, top_count, col_width)
    routed = jnp.sum(picked * route_weight[:, :, None], axis=1)
    shared_cols = jnp.dot(gathered_shared, shared_down, preferred_element_type=jnp.float32)
    return (updated_cols.astype(jnp.float32) + shared_cols + routed).astype(jnp.bfloat16)


def solution(mesh):
    torus = Mesh(
        mesh.devices.reshape(mesh.shape["grp"], 16, 2, mesh.shape["tp"]),
        ("grp", "sp_0", "sp_1", "tp"),
    )
    in_specs = (
        P(GRP_SP, None),
        P(GRP_SP, "tp"),
        P(GRP_SP, "tp"),
        P(GRP_SP, "tp"),
        P(GRP_SP),
        P(GRP_SP, None),
        P(GRP_SP, None),
        P("tp"),
        P("tp", None),
        P(),
        P(SP, None, "tp"),
        P(SP, None, "tp"),
        P(SP, None, "tp"),
        P(None, "tp"),
        P(None, "tp"),
        P(None, "tp"),
    )
    out_specs = P(GRP_SP, "tp")
    return jax.shard_map(
        shards, mesh=torus, in_specs=in_specs, out_specs=out_specs, check_vma=False
    )
```

profile of v0, /device:TPU:65, one launch (start us, length us, event | category | flops | bytes accessed | tf_op | source)
XLA Modules:
  0.0 356.7 jit_solution(9728244078039882902)
XLA Ops:
  6.6 0.7 bitcast_convert_fusion
  7.3 7.1 %collective-permute-start.1 = (bf16[128]{0:T(256)(128)(2,1)S(1)}, bf16[128]{0:T(256)(128)(2,1)S(1)}, u32[]{:S(2)}, u32[]{:S(2)}) collective-permute-start(bf16[128]{0:T(256)(128)(2,1)S(1)} %slice.57), channel_id=1, source_target_pairs={{0,8},{8,16},{16,24},{24,32},{32,40},{40,48},{48,56},{56,64},{64,7... | collective-permute-start | bytes 776 | tf_op jit(solution)/shard_map/ppermute | solution.py:19
  15.1 1.9 collective-permute-start.2
  17.8 6.1 %collective-permute-start = (bf16[128,64]{0,1:T(8,128)(2,1)S(1)}, bf16[128,64]{0,1:T(8,128)(2,1)S(1)}, u32[]{:S(2)}, u32[]{:S(2)}) collective-permute-start(bf16[128,64]{0,1:T(8,128)(2,1)S(1)} %slice.53), channel_id=1, source_target_pairs={{0,8},{8,16},{16,24},{24,32},{32,40},{40,48},{48,56},{56,64},{64,7... | collective-permute-start | bytes 49160 | tf_op jit(solution)/shard_map/ppermute | solution.py:19
  23.9 0.8 copy_bitcast_fusion
  24.7 0.8 copy_bitcast_fusion.2
  25.5 0.9 reshape.250
  26.4 24.3 %collective-permute-done.1 = bf16[128]{0:T(256)(128)(2,1)S(1)} collective-permute-done((bf16[128]{0:T(256)(128)(2,1)S(1)}, bf16[128]{0:T(256)(128)(2,1)S(1)}, u32[]{:S(2)}, u32[]{:S(2)}) %collective-permute-start.1) | collective-permute-done | bytes 288 | tf_op jit(solution)/shard_map/ppermute | solution.py:19
  50.8 1.9 collective-permute-done.2
  54.6 0.7 exponential_add_fusion
  56.9 1.1 copy.79
  57.9 3.8 %all-to-all-start = ((bf16[8,256,256]{2,1,0:T(8,128)(2,1)}), bf16[8,256,256]{2,1,0:T(8,128)(2,1)S(1)}, u32[]{:S(2)}, u32[]{:S(2)}) async-start(bf16[8,256,256]{2,1,0:T(8,128)(2,1)} %bitcast.106), calls=%async_computation | async-start | bytes 2097152 | tf_op jit(solution)/shard_map/all_to_all | solution.py:30
  62.5 1.2 reduce-window.6
  64.1 2.4 scatter_custom_fusion
  66.7 0.8 dynamic_slice.7
  67.4 19.8 %all-to-all-done = bf16[8,256,256]{2,1,0:T(8,128)(2,1)S(1)} async-done(((bf16[8,256,256]{2,1,0:T(8,128)(2,1)}), bf16[8,256,256]{2,1,0:T(8,128)(2,1)S(1)}, u32[]{:S(2)}, u32[]{:S(2)}) %all-to-all-start) | async-done | bytes 1048608 | tf_op jit(solution)/shard_map/all_to_all | solution.py:30
  87.4 1.0 fusion.17
  88.4 11.1 %psum.7 = f32[256]{0:T(256)S(1)} all-reduce(f32[256]{0:T(256)S(1)} %get-tuple-element.5), channel_id=1, replica_groups=mesh['grp'=2,'sp_0'=16,'sp_1'=2,'tp'=8] {'tp'}, use_global_device_ids=true, to_apply=%region_8.9 | all-reduce | flops 256 | bytes 2048 | tf_op jit(solution)/shard_map/psum | solution.py:152
  99.6 3.9 %gather_fusion = bf16[1024,256]{1,0:T(8,128)(2,1)S(1)} fusion(bf16[256,256]{1,0:T(8,128)(2,1)S(1)} %fusion.19, s32[1024]{0:T(1024)S(1)} %fusion.37), kind=kCustom, calls=%fused_computation | custom fusion | bytes 1052672 | tf_op jit(solution)/shard_map/gather | solution.py:171
  103.8 11.5 %all_to_all.25 = bf16[16,2,1,32,256]{4,3,0,2,1:T(8,128)(2,1)S(1)} all-to-all(bf16[16,2,1,32,256]{4,3,0,2,1:T(8,128)(2,1)S(1)} %copy_select_fusion), channel_id=1, replica_groups=mesh['grp'=2,'sp_0'=16,'sp_1'=2,'tp'=8] {'sp_1'}, dimensions={1} | all-to-all | bytes 1048576 | tf_op jit(solution)/shard_map/all_to_all | solution.py:56
  115.3 36.5 %all_to_all.26 = bf16[16,2,1,32,256]{4,3,1,2,0:T(8,128)(2,1)} all-to-all(bf16[16,2,1,32,256]{4,3,1,2,0:T(8,128)(2,1)S(1)} %copy.49), channel_id=1, replica_groups=mesh['grp'=2,'sp_0'=16,'sp_1'=2,'tp'=8] {'sp_0'}, dimensions={0} | all-to-all | bytes 1048576 | tf_op jit(solution)/shard_map/all_to_all | solution.py:56
  152.2 24.5 %all_to_all.27 = bf16[8,256,256]{1,2,0:T(8,128)(2,1)S(1)} all-to-all(bf16[8,256,256]{1,2,0:T(8,128)(2,1)S(1)} %broadcast_in_dim.70), channel_id=1, replica_groups=mesh['grp'=2,'sp_0'=16,'sp_1'=2,'tp'=8] {'tp'}, dimensions={0} | all-to-all | bytes 2097152 | tf_op jit(solution)/shard_map/all_to_all | solution.py:36
  177.6 47.7 %all-gather.3.cloned.1.call-done = bf16[32,32,2048]{2,1,0:T(8,128)(2,1)} async-done(((bf16[32,32,256]{2,1,0:T(8,128)(2,1)}), bf16[32,32,2048]{2,1,0:T(8,128)(2,1)}) %all-gather.3.cloned.1.call-update) | async-done | bytes 4194320 | tf_op jit(solution)/shard_map/all_gather | solution.py:175
  225.3 3.6 %fusion.14 = f32[1024,128]{1,0:T(8,128)S(1)} fusion(bf16[1024,2048]{1,0:T(8,128)(2,1)} %bitcast.108, bf16[1,2048,128]{2,1,0:T(8,128)(2,1)S(1)} %copy-done.2), kind=kOutput, calls=%fused_computation.23 | convolution fusion | flops 536870912 | bytes 5242880 | tf_op jit(solution)/shard_map/dot_general | solution.py:177
  229.0 1.2 fusion.6
  230.2 0.7 pad_maximum_fusion
  231.0 59.2 %all-gather.5.cloned.1.call-done = bf16[1280,1024]{1,0:T(8,128)(2,1)} async-done(((bf16[1280,128]{1,0:T(8,128)(2,1)}), bf16[1280,1024]{1,0:T(8,128)(2,1)}) %all-gather.5.cloned.1.call-update) | async-done | bytes 2621456 | tf_op jit(solution)/shard_map/all_gather | solution.py:72
  290.2 3.1 fusion.2
  293.3 18.3 %all-to-all-start.4 = ((bf16[32,32,256]{2,1,0:T(8,128)(2,1)}), bf16[32,32,256]{2,1,0:T(8,128)(2,1)S(1)}, u32[]{:S(2)}, u32[]{:S(2)}) async-start(bf16[32,32,256]{2,1,0:T(8,128)(2,1)} %bitcast.25), calls=%async_computation.4 | async-start | bytes 1048576 | tf_op jit(solution)/shard_map/all_to_all | solution.py:184
  311.8 33.1 %all-to-all-done.4 = bf16[32,32,256]{2,1,0:T(8,128)(2,1)S(1)} async-done(((bf16[32,32,256]{2,1,0:T(8,128)(2,1)}), bf16[32,32,256]{2,1,0:T(8,128)(2,1)S(1)}, u32[]{:S(2)}, u32[]{:S(2)}) %all-to-all-start.4) | async-done | bytes 524320 | tf_op jit(solution)/shard_map/all_to_all | solution.py:184
  344.9 1.9 gather_fusion.1
  347.9 2.0 fusion.8
  (72 shorter events, 9.2 us)
Async XLA Ops:
  6.5 49.8 %copy-start = (bf16[128,2048]{1,0:T(8,128)(2,1)S(1)}, bf16[128,2048]{1,0:T(8,128)(2,1)}, u32[]{:S(2)}) copy-start(bf16[128,2048]{1,0:T(8,128)(2,1)} %param.24) | copy-start | bytes 1572868
  7.3 43.4 %collective-permute-start.1 = (bf16[128]{0:T(256)(128)(2,1)S(1)}, bf16[128]{0:T(256)(128)(2,1)S(1)}, u32[]{:S(2)}, u32[]{:S(2)}) collective-permute-start(bf16[128]{0:T(256)(128)(2,1)S(1)} %slice.57), channel_id=1, source_target_pairs={{0,8},{8,16},{16,24},{24,32},{32,40},{40,48},{48,56},{56,64},{64,7... | collective-permute-start | bytes 776 | tf_op jit(solution)/shard_map/ppermute | solution.py:19
  15.1 37.6 %collective-permute-start.2 = (bf16[128,64]{0,1:T(8,128)(2,1)S(1)}, bf16[128,64]{0,1:T(8,128)(2,1)S(1)}, u32[]{:S(2)}, u32[]{:S(2)}) collective-permute-start(bf16[128,64]{0,1:T(8,128)(2,1)S(1)} %slice.60), channel_id=1, source_target_pairs={{0,8},{8,16},{16,24},{24,32},{32,40},{40,48},{48,56},{56,64},{64,7... | collective-permute-start | bytes 49160 | tf_op jit(solution)/shard_map/ppermute | solution.py:19
  17.8 37.6 %collective-permute-start = (bf16[128,64]{0,1:T(8,128)(2,1)S(1)}, bf16[128,64]{0,1:T(8,128)(2,1)S(1)}, u32[]{:S(2)}, u32[]{:S(2)}) collective-permute-start(bf16[128,64]{0,1:T(8,128)(2,1)S(1)} %slice.53), channel_id=1, source_target_pairs={{0,8},{8,16},{16,24},{24,32},{32,40},{40,48},{48,56},{56,64},{64,7... | collective-permute-start | bytes 49160 | tf_op jit(solution)/shard_map/ppermute | solution.py:19
  56.4 5.4 %copy-start.5 = (s32[256,2]{0,1:T(2,128)S(1)}, s32[256,2]{0,1:T(2,128)}, u32[]{:S(2)}) copy-start(s32[256,2]{0,1:T(2,128)} %param.21) | copy-start | bytes 6148
  57.9 29.3 %all-to-all-start = ((bf16[8,256,256]{2,1,0:T(8,128)(2,1)}), bf16[8,256,256]{2,1,0:T(8,128)(2,1)S(1)}, u32[]{:S(2)}, u32[]{:S(2)}) async-start(bf16[8,256,256]{2,1,0:T(8,128)(2,1)} %bitcast.106), calls=%async_computation | async-start | bytes 2097152 | tf_op jit(solution)/shard_map/all_to_all | solution.py:30
  61.7 163.6 %all-gather.3.cloned.1.call-start = ((), (), s32[]{:S(2)}) async-start(), calls=%async_computation.5 | async-start | bytes 4718592 | tf_op jit(solution)/shard_map/all_gather | solution.py:175
  115.3 61.3 %copy-start.4 = (bf16[2048,128]{1,0:T(8,128)(2,1)S(1)}, bf16[2048,128]{1,0:T(8,128)(2,1)}, u32[]{:S(2)}) copy-start(bf16[2048,128]{1,0:T(8,128)(2,1)} %param.29) | copy-start | bytes 1572868
  151.9 25.2 %copy-start.7 = (bf16[2048,128]{1,0:T(8,128)(2,1)S(1)}, bf16[2048,128]{1,0:T(8,128)(2,1)}, u32[]{:S(2)}) copy-start(bf16[2048,128]{1,0:T(8,128)(2,1)} %param.30) | copy-start | bytes 1572868
  151.9 138.3 %all-gather.5.cloned.1.call-start = ((), (), s32[]{:S(2)}) async-start(), calls=%async_computation.6 | async-start | bytes 2949120 | tf_op jit(solution)/shard_map/all_gather | solution.py:72
  152.1 73.2 %copy-start.2 = (bf16[1,2048,128]{2,1,0:T(8,128)(2,1)S(1)}, bf16[1,2048,128]{2,1,0:T(8,128)(2,1)}, u32[]{:S(2)}) copy-start(bf16[1,2048,128]{2,1,0:T(8,128)(2,1)} %param.26) | copy-start | bytes 1572868
  225.3 3.6 %copy-start.1 = (bf16[32,32,2048]{2,1,0:T(8,128)(2,1)S(1)}, bf16[32,32,2048]{2,1,0:T(8,128)(2,1)}, u32[]{:S(2)}) copy-start(bf16[32,32,2048]{2,1,0:T(8,128)(2,1)} %all-gather.3.cloned.1.call-done) | copy-start | bytes 12582916
  225.3 3.6 %copy-start.8 = (bf16[1,2048,128]{2,1,0:T(8,128)(2,1)S(1)}, bf16[1,2048,128]{2,1,0:T(8,128)(2,1)}, u32[]{:S(2)}) copy-start(bf16[1,2048,128]{2,1,0:T(8,128)(2,1)} %param.27) | copy-start | bytes 1572868
  229.0 61.2 %copy-start.9 = (bf16[1,1024,256]{2,1,0:T(8,128)(2,1)S(1)}, bf16[1,1024,256]{2,1,0:T(8,128)(2,1)}, u32[]{:S(2)}) copy-start(bf16[1,1024,256]{2,1,0:T(8,128)(2,1)} %param.28) | copy-start | bytes 1572868
  231.0 80.6 %copy-start.6 = (f32[256,2]{0,1:T(2,128)S(1)}, f32[256,2]{0,1:T(2,128)}, u32[]{:S(2)}) copy-start(f32[256,2]{0,1:T(2,128)} %param.22) | copy-start | bytes 6148
  293.3 54.6 %copy-start.3 = (bf16[1024,256]{1,0:T(8,128)(2,1)S(1)}, bf16[1024,256]{1,0:T(8,128)(2,1)}, u32[]{:S(2)}) copy-start(bf16[1024,256]{1,0:T(8,128)(2,1)} %param.31) | copy-start | bytes 1572868
  293.3 51.6 %all-to-all-start.4 = ((bf16[32,32,256]{2,1,0:T(8,128)(2,1)}), bf16[32,32,256]{2,1,0:T(8,128)(2,1)S(1)}, u32[]{:S(2)}, u32[]{:S(2)}) async-start(bf16[32,32,256]{2,1,0:T(8,128)(2,1)} %bitcast.25), calls=%async_computation.4 | async-start | bytes 1048576 | tf_op jit(solution)/shard_map/all_to_all | solution.py:184
Sparse Core Ops, SparseCore 0:
  152.0 73.2 all-gather.2
  231.1 59.0 all-gather.4
where the time goes:
time: 358 us; the launch traced here: 357 us
  waiting for transfers between devices  186 us (52%)
  blocking collectives  83.5 us (23%)
  starting transfers between devices  37.3 us (10%)
  local copies, waits for them, and re-layouts  15.8 us (4%)
  between operations  13.8 us (4%)
  matrix products  11.9 us (3%)
  other arithmetic  8.26 us (2%)
    all_gather x1, waiting for transfers between devices, sent_together(): lax.all_gather(both, axis, axis=dim, tiled=True)  59.2 us
    all_to_all x2, blocking collectives, moved_by_axis(): lax.all_to_all(blocks, axes[k], split_axis=k, concat_axis=k, tiled=True)  48 us
    all_gather x1, waiting for transfers between devices, shards(): arrived = lax.all_gather(pieces, 'tp', axis=2, tiled=True)  47.7 us
    all_to_all x1, waiting for transfers between devices, shards(): lax.all_to_all(expert_out.reshape(experts, capacity, col_width), SP, spli...  33.1 us
    ppermute x3, waiting for transfers between devices, passed_along(): lax.ppermute(value, axis, [(source, source + steps) for source in range(l...  26.1 us
    all_to_all x1, blocking collectives, sent_to_all(): lax.all_to_all(jnp.broadcast_to(array[None], (size, *array.shape)), axis,...  24.5 us
    all_to_all x1, waiting for transfers between devices, sent_and_summed(): blocks = lax.all_to_all(split_up(array, dim, size), axis, 0, 0, tiled=True)  19.8 us
    all_to_all x1, starting transfers between devices, shards(): lax.all_to_all(expert_out.reshape(experts, capacity, col_width), SP, spli...  18.3 us
  transfers between devices with their start and end apart: 7, of which 6 were waited for; matrix products, arithmetic and copies ran while one was open for 4% of the time, Pallas kernels for 0%

commit v1 on v0

v1 whole, which is shorter than its diff:
```python
import functools

import jax
import jax.numpy as jnp
from jax import lax
from jax.experimental import pallas as pl
from jax.experimental.pallas import tpu as pltpu
from jax.sharding import PartitionSpec as P

HEAD_DIM = 64
WINDOW = 128
CORES = 2
GRP_SP = ("grp", "sp")
EPSILON = 1e-06
MESH = pl.DeviceIdType.MESH
BF16 = jnp.bfloat16
F32 = jnp.float32


def delta_order(nz):
    far = sorted((d if d <= nz // 2 else d - nz for d in range(nz)), key=lambda d: (-abs(d), -d))
    first = [d for d in far if abs(d) == nz // 4]
    return first + [d for d in far if d not in first]


class Ring:
    def __init__(self, n, me, buf, send_sem, recv_sem):
        self.n, self.me, self.buf, self.send_sem, self.recv_sem = n, me, buf, send_sem, recv_sem

    def hops(self, turn, right):
        longer = self.n // 2
        return longer if right == (turn % 2 == 0) else self.n - 1 - longer

    def copy(self, rows, index, right, hop):
        step = 1 if right else -1
        origin = lax.rem(self.me - step * (hop - 1) + self.n, self.n)
        target = lax.rem(self.me + step + self.n, self.n)
        ref = self.buf.at[origin, rows]
        return pltpu.make_async_remote_copy(
            src_ref=ref,
            dst_ref=ref,
            send_sem=self.send_sem,
            recv_sem=self.recv_sem.at[index, 0 if right else 1, hop - 1],
            device_id={"tp": target},
            device_id_type=MESH,
        )

    def arrival(self, rows, index, right, hop):
        step = 1 if right else -1
        origin = lax.rem(self.me - step * hop + self.n, self.n)
        ref = self.buf.at[origin, rows]
        pltpu.make_async_remote_copy(
            src_ref=ref,
            dst_ref=ref,
            send_sem=self.send_sem,
            recv_sem=self.recv_sem.at[index, 0 if right else 1, hop - 1],
            device_id={"tp": self.me},
            device_id_type=MESH,
        ).wait_recv()

    def begin(self, rows, index):
        for right in (True, False):
            if self.hops(index, right) > 0:
                self.copy(rows, index, right, 1).start()

    def pass_on(self, rows, index, hop):
        for right in (True, False):
            most = self.hops(index, right)
            if hop <= most:
                self.arrival(rows, index, right, hop)
                if hop < most:
                    self.copy(rows, index, right, hop + 1).start()

    def longest(self):
        return self.n // 2

    def finish(self):
        ref = self.buf.at[pl.ds(0, self.n - 1)]
        pltpu.make_async_remote_copy(
            src_ref=ref,
            dst_ref=ref,
            send_sem=self.send_sem,
            recv_sem=self.recv_sem.at[0, 0, 0],
            device_id={"tp": self.me},
            device_id_type=MESH,
        ).wait_send()


def layer(
    nsp,
    ntp,
    cap,
    residual,
    queries,
    keys,
    values,
    meta,
    sinks,
    out_weight,
    gain,
    expert_gate,
    expert_up,
    expert_down,
    shared_gate,
    shared_up,
    shared_down,
    out,
    halo_k,
    halo_v,
    halo_m,
    proj_w,
    res,
    att,
    upd,
    normed,
    scatter,
    pick,
    outgoing,
    rows_all,
    act_all,
    made,
    back,
    expert_in,
    expert_out,
    shared_in,
    shared_out,
    halo_send,
    halo_recv,
    w_send,
    w_recv,
    pair_send,
    pair_recv,
    att_send,
    att_recv,
    upd_send,
    upd_recv,
    disp_send,
    disp_recv,
    rows_send,
    rows_recv,
    act_send,
    act_recv,
    ret_send,
    ret_recv,
    load_sem,
):
    me = lax.axis_index("sp")
    tp = lax.axis_index("tp")
    nz = nsp // CORES
    z, core = me // CORES, lax.rem(me, CORES)
    tokens = queries.shape[0]
    cols = res.shape[1]
    heads_wide = queries.shape[1]
    blocks = tokens // WINDOW
    slots = nsp * cap
    hidden = expert_gate.shape[2]
    sibling = z * CORES + lax.rem(core + 1, CORES)
    following = lax.rem(me + 1, nsp)

    col_start = pl.multiple_of(tp * cols, cols)
    loads = [
        (residual.at[:, pl.ds(col_start, cols)], res),
        (shared_gate, shared_in.at[:, pl.ds(0, hidden)]),
        (shared_up, shared_in.at[:, pl.ds(hidden, hidden)]),
        (expert_gate.at[0], expert_in.at[:, pl.ds(0, hidden)]),
        (expert_up.at[0], expert_in.at[:, pl.ds(hidden, hidden)]),
        (expert_down.at[0], expert_out),
        (shared_down, shared_out),
    ]
    loads = [pltpu.make_async_copy(src, dst, load_sem.at[i]) for i, (src, dst) in enumerate(loads)]
    for load in loads:
        load.start()

    barrier = pltpu.get_barrier_semaphore()
    for d in range(1, nsp):
        pl.semaphore_signal(
            barrier, inc=1, device_id={"sp": lax.rem(me + d, nsp)}, device_id_type=MESH
        )
    for d in range(1, ntp):
        pl.semaphore_signal(
            barrier, inc=1, device_id={"tp": lax.rem(tp + d, ntp)}, device_id_type=MESH
        )
    pl.semaphore_wait(barrier, nsp - 1 + ntp - 1)

    tail = pl.ds(tokens - WINDOW, WINDOW)
    halo = [
        pltpu.make_async_remote_copy(
            src_ref=src,
            dst_ref=dst,
            send_sem=halo_send.at[i],
            recv_sem=halo_recv.at[i],
            device_id={"sp": following},
            device_id_type=MESH,
        )
        for i, (src, dst) in enumerate(
            [(keys.at[tail], halo_k), (values.at[tail], halo_v), (meta.at[:, tail], halo_m)]
        )
    ]
    for copy in halo:
        copy.start()

    part = heads_wide // CORES

    def weight_copy(d):
        target = lax.rem(tp + d, ntp)
        return pltpu.make_async_remote_copy(
            src_ref=out_weight.at[
                pl.ds(pl.multiple_of(core * part, part), part),
                pl.ds(pl.multiple_of(target * cols, cols), cols),
            ],
            dst_ref=proj_w.at[pl.ds(pl.multiple_of(tp * heads_wide + core * part, part), part)],
            send_sem=w_send.at[d - 1],
            recv_sem=w_recv.at[d - 1],
            device_id={"tp": target},
            device_id_type=MESH,
        )

    def weight_rows(d, which):
        source = lax.rem(tp - d + ntp, ntp)
        return proj_w.at[pl.ds(pl.multiple_of(source * heads_wide + which * part, part), part)]

    def pair_copy(d):
        ref = weight_rows(d, core)
        return pltpu.make_async_remote_copy(
            src_ref=ref,
            dst_ref=ref,
            send_sem=pair_send.at[d - 1],
            recv_sem=pair_recv.at[d - 1],
            device_id={"sp": sibling},
            device_id_type=MESH,
        )

    distances = sorted(range(1, ntp), key=lambda d: min(d, ntp - d))
    for d in distances:
        weight_copy(d).start()
    proj_w[pl.ds(pl.multiple_of(tp * heads_wide, heads_wide), heads_wide), :] = out_weight[
        :, pl.ds(col_start, cols)
    ]

    att_ring = Ring(ntp, tp, att, att_send, att_recv)
    upd_ring = Ring(ntp, tp, upd, upd_send, upd_recv)
    row_meta = meta[...]
    col_meta = jnp.transpose(row_meta)
    q_pos = lax.broadcasted_iota(jnp.int32, (WINDOW, 2 * WINDOW), 0)
    k_pos = lax.broadcasted_iota(jnp.int32, (WINDOW, 2 * WINDOW), 1)
    offset = q_pos + WINDOW - k_pos
    band = (offset >= 0) & (offset < WINDOW)

    def attend(b, band_k, band_v, band_seg):
        rows = slice(b * WINDOW, (b + 1) * WINDOW)
        allowed = band & (col_meta[rows, 0:1] == band_seg)
        heads = []
        for h in range(heads_wide // HEAD_DIM):
            q = queries[rows, h * HEAD_DIM : (h + 1) * HEAD_DIM]
            scores = lax.dot_general(
                q, band_k, (((1,), (1,)), ((), ())), preferred_element_type=F32
            ) * HEAD_DIM ** (-0.5)
            masked = jnp.where(allowed, scores, -jnp.inf)
            sink = sinks[h]
            top = jnp.maximum(jnp.max(masked, axis=-1, keepdims=True), sink)
            terms = jnp.exp(masked - top)
            denominator = jnp.sum(terms, axis=-1, keepdims=True) + jnp.exp(sink - top)
            weights = (terms / denominator).astype(BF16)
            heads.append(jnp.dot(weights, band_v, preferred_element_type=F32).astype(BF16))
        att[tp, rows, :] = jnp.concatenate(heads, axis=1)

    order = list(range(1, blocks)) + [0]
    span = [pl.ds(b * WINDOW, WINDOW) for b in range(blocks)]
    for b in order[:-1]:
        reach = slice((b - 1) * WINDOW, (b + 1) * WINDOW)
        attend(b, keys[reach, :], values[reach, :], row_meta[0:1, reach])
        att_ring.begin(span[b], b)
    for copy in halo:
        copy.wait_recv()
    halo_seg = jnp.where(me == 0, -1.0, halo_m[0:1, :])
    attend(
        0,
        jnp.concatenate([halo_k[...], keys[0:WINDOW, :]], axis=0),
        jnp.concatenate([halo_v[...], values[0:WINDOW, :]], axis=0),
        jnp.concatenate([halo_seg, row_meta[0:1, 0:WINDOW]], axis=1),
    )
    att_ring.begin(span[0], 0)

    route_of = [row_meta[1 + k : 2 + k, :] for k in range(2)]
    experts = lax.broadcasted_iota(jnp.int32, (nsp, tokens), 0).astype(F32)
    named = [(experts == r).astype(F32) for r in route_of]
    earlier = lax.broadcasted_iota(jnp.int32, (tokens, tokens), 0)
    later = lax.broadcasted_iota(jnp.int32, (tokens, tokens), 1)
    before = (earlier < later).astype(F32).astype(BF16)
    counts = jnp.dot((named[0] + named[1]).astype(BF16), before, preferred_element_type=F32)
    slot_row = [
        r * cap + jnp.sum(counts * m, axis=0, keepdims=True) for r, m in zip(route_of, named)
    ]
    slot_down = lax.broadcasted_iota(jnp.int32, (slots, tokens), 0).astype(F32)
    hit = (slot_down == slot_row[0]) | (slot_down == slot_row[1])
    scatter[...] = jnp.where(hit, 1.0, 0.0).astype(BF16)
    slot_col = jnp.transpose(
        jnp.concatenate([slot_row[0], slot_row[1], jnp.zeros((6, tokens), F32)], axis=0)
    )
    slot_along = lax.broadcasted_iota(jnp.int32, (tokens, slots), 1).astype(F32)
    for k in range(2):
        pick[k, :, :] = jnp.where(slot_along == slot_col[:, k : k + 1], 1.0, 0.0).astype(BF16)

    def weight_arrival(d):
        weight_copy(d).wait_recv()
        pair_copy(d).start()

    for hop in range(1, att_ring.longest() + 1):
        for b in order:
            att_ring.pass_on(span[b], b, hop)
        if hop == 1:
            for d in distances:
                weight_arrival(d)
    for d in distances:
        pair_copy(d).wait_recv()
    loads[0].wait()

    for b in order:
        rows = slice(b * WINDOW, (b + 1) * WINDOW)
        total = jnp.zeros((WINDOW, cols), F32)
        for s in range(ntp):
            total += jnp.dot(
                att[s, rows, :],
                proj_w[s * heads_wide : (s + 1) * heads_wide, :],
                preferred_element_type=F32,
            )
        upd[tp, rows, :] = (res[rows, :].astype(F32) + total).astype(BF16)
        upd_ring.begin(span[b], b)
    for hop in range(1, upd_ring.longest() + 1):
        for b in order:
            upd_ring.pass_on(span[b], b, hop)

    squares = jnp.zeros((tokens, 1), F32)
    for s in range(ntp):
        part_rows = upd[s].astype(F32)
        squares += jnp.sum(part_rows * part_rows, axis=-1, keepdims=True)
    inv_rms = lax.rsqrt(squares / (ntp * cols) + EPSILON)
    for s in range(ntp):
        normed[s] = (upd[s].astype(F32) * inv_rms * gain[s : s + 1, :]).astype(BF16)

    deltas = delta_order(nz)
    places = [(d, s) for d in deltas for s in range(CORES)]
    outgoing[...] = jnp.dot(scatter[...], normed[tp], preferred_element_type=F32).astype(BF16)

    def at_chip(d, s):
        return lax.rem(z + d + nz, nz) * CORES + lax.rem(core + s, CORES)

    def slot_block(index):
        return pl.ds(pl.multiple_of(index * cap, cap), cap)

    def dispatch_copy(i):
        d, s = places[i]
        target = at_chip(-d, s)
        return pltpu.make_async_remote_copy(
            src_ref=outgoing.at[slot_block(target)],
            dst_ref=rows_all.at[tp, pl.ds(i * cap, cap)],
            send_sem=disp_send,
            recv_sem=disp_recv.at[i],
            device_id={"sp": target},
            device_id_type=MESH,
        )

    own_place = places.index((0, 0))
    for i in range(nsp):
        if i != own_place:
            dispatch_copy(i).start()
    rows_all[tp, own_place * cap : (own_place + 1) * cap, :] = outgoing[slot_block(me), :]

    act_ring = Ring(ntp, tp, act_all, act_send, act_recv)
    rows_ring = Ring(ntp, tp, rows_all, rows_send, rows_recv)

    def activate(gate_up):
        gate, up = gate_up[:, :hidden], gate_up[:, hidden:]
        return (gate / (1.0 + jnp.exp(-gate)) * up).astype(BF16)

    for load in loads[1:]:
        load.wait()
    total = jnp.zeros((tokens, 2 * hidden), F32)
    for s in range(ntp):
        total += jnp.dot(
            normed[s], shared_in[s * cols : (s + 1) * cols, :], preferred_element_type=F32
        )
    act_all[tp, slots : slots + tokens, :] = activate(total)
    chunk_places = 2 * CORES
    chunks = nsp // chunk_places
    chunk = chunk_places * cap
    shared_span = pl.ds(slots, tokens)
    act_ring.begin(shared_span, chunks)

    def ready(q):
        for i in range(q * chunk_places, (q + 1) * chunk_places):
            if i != own_place:
                dispatch_copy(i).wait_recv()
        rows_ring.begin(pl.ds(q * chunk, chunk), q)

    def rows_hop(q, hop):
        rows_ring.pass_on(pl.ds(q * chunk, chunk), q, hop)

    def hidden_units(q):
        rows = slice(q * chunk, (q + 1) * chunk)
        total = jnp.zeros((chunk, 2 * hidden), F32)
        for s in range(ntp):
            total += jnp.dot(
                rows_all[s, rows, :],
                expert_in[s * cols : (s + 1) * cols, :],
                preferred_element_type=F32,
            )
        act_all[tp, rows, :] = activate(total)
        act_ring.begin(pl.ds(q * chunk, chunk), q)

    def act_hop(q, hop):
        act_ring.pass_on(pl.ds(q * chunk, chunk), q, hop)

    def shared_hop(hop):
        act_ring.pass_on(shared_span, chunks, hop)

    def return_copy(i):
        d, s = places[i]
        target = at_chip(d, s)
        return pltpu.make_async_remote_copy(
            src_ref=made.at[pl.ds(i * cap, cap)],
            dst_ref=back.at[slot_block(me)],
            send_sem=ret_send,
            recv_sem=ret_recv.at[i],
            device_id={"sp": target},
            device_id_type=MESH,
        )

    def outputs(q):
        rows = slice(q * chunk, (q + 1) * chunk)
        total = jnp.zeros((chunk, cols), F32)
        for s in range(ntp):
            total += jnp.dot(
                act_all[s, rows, :],
                expert_out[s * hidden : (s + 1) * hidden, :],
                preferred_element_type=F32,
            )
        made[rows, :] = total.astype(BF16)
        for i in range(q * chunk_places, (q + 1) * chunk_places):
            if i == own_place:
                back[slot_block(me), :] = made[i * cap : (i + 1) * cap, :]
            else:
                return_copy(i).start()

    period, row_hop, act_hop_time = 7.3, 4.0, 3.2
    head = 4.0
    longest = rows_ring.longest()
    steps = []
    for hop in range(1, longest + 1):
        steps.append((hop * 4.0, functools.partial(shared_hop, hop)))
    for q in range(chunks):
        at = head + q * period
        steps.append((at, functools.partial(ready, q)))
        for hop in range(1, longest + 1):
            steps.append((at + hop * row_hop, functools.partial(rows_hop, q, hop)))
        at += longest * row_hop + 0.1
        steps.append((at, functools.partial(hidden_units, q)))
        for hop in range(1, longest + 1):
            steps.append((at + hop * act_hop_time, functools.partial(act_hop, q, hop)))
        at += longest * act_hop_time + 0.1
        steps.append((at, functools.partial(outputs, q)))
    for _, step in sorted(steps, key=lambda step: step[0]):
        step()

    total = upd[tp].astype(F32)
    for s in range(ntp):
        total += jnp.dot(
            act_all[s, slots : slots + tokens, :],
            shared_out[s * hidden : (s + 1) * hidden, :],
            preferred_element_type=F32,
        )
    for i in range(nsp):
        if i != own_place:
            d, s = places[i]
            source = at_chip(-d, s)
            ref = back.at[slot_block(source)]
            pltpu.make_async_remote_copy(
                src_ref=ref,
                dst_ref=ref,
                send_sem=ret_send,
                recv_sem=ret_recv.at[i],
                device_id={"sp": source},
                device_id_type=MESH,
            ).wait_recv()
    for k in range(2):
        picked = jnp.dot(pick[k], back[...], preferred_element_type=F32)
        total += picked * col_meta[:, 3 + k : 4 + k]
    out[...] = total.astype(BF16)

    for copy in halo:
        copy.wait_send()
    for d in distances:
        weight_copy(d).wait_send()
        pair_copy(d).wait_send()
    for ring in (att_ring, upd_ring, rows_ring, act_ring):
        ring.finish()
    most = pl.ds(0, (nsp - 1) * cap)
    for buffer, sem in ((outgoing, disp_send), (made, ret_send)):
        ref = buffer.at[most]
        pltpu.make_async_remote_copy(
            src_ref=ref,
            dst_ref=ref,
            send_sem=sem,
            recv_sem=ret_recv.at[0],
            device_id={"sp": me},
            device_id_type=MESH,
        ).wait_send()


def shards(
    nsp,
    ntp,
    residual,
    queries,
    keys,
    values,
    segments,
    routes,
    route_weight,
    sinks,
    out_weight,
    norm_gain,
    expert_gate,
    expert_up,
    expert_down,
    shared_gate,
    shared_up,
    shared_down,
):
    tokens, width = residual.shape
    cols = width // ntp
    hidden = expert_gate.shape[2]
    heads_wide = queries.shape[1]
    cap = 2 * tokens * routes.shape[1] // nsp
    slots = nsp * cap
    chunks = nsp // (2 * CORES)
    longest = ntp // 2
    meta = jnp.concatenate(
        [
            segments[None].astype(F32),
            routes.T.astype(F32),
            route_weight.T,
            jnp.zeros((3, tokens), F32),
        ],
        axis=0,
    )
    vmem = pl.BlockSpec(memory_space=pltpu.VMEM)
    smem = pl.BlockSpec(memory_space=pltpu.SMEM)
    anywhere = pl.BlockSpec(memory_space=pl.ANY)
    dma = pltpu.SemaphoreType.DMA
    return pl.pallas_call(
        functools.partial(layer, nsp, ntp, cap),
        out_shape=jax.ShapeDtypeStruct((tokens, cols), BF16),
        in_specs=[anywhere, vmem, vmem, vmem, vmem, smem, vmem, vmem] + [anywhere] * 6,
        out_specs=vmem,
        scratch_shapes=[
            pltpu.VMEM((WINDOW, keys.shape[1]), BF16),
            pltpu.VMEM((WINDOW, values.shape[1]), BF16),
            pltpu.VMEM((8, WINDOW), F32),
            pltpu.VMEM((ntp * heads_wide, cols), BF16),
            pltpu.VMEM((tokens, cols), BF16),
            pltpu.VMEM((ntp, tokens, heads_wide), BF16),
            pltpu.VMEM((ntp, tokens, cols), BF16),
            pltpu.VMEM((ntp, tokens, cols), BF16),
            pltpu.VMEM((slots, tokens), BF16),
            pltpu.VMEM((2, tokens, slots), BF16),
            pltpu.VMEM((slots, cols), BF16),
            pltpu.VMEM((ntp, slots, cols), BF16),
            pltpu.VMEM((ntp, slots + tokens, hidden), BF16),
            pltpu.VMEM((slots, cols), BF16),
            pltpu.VMEM((slots, cols), BF16),
            pltpu.VMEM((width, 2 * hidden), BF16),
            pltpu.VMEM((ntp * hidden, cols), BF16),
            pltpu.VMEM((width, 2 * hidden), BF16),
            pltpu.VMEM((ntp * hidden, cols), BF16),
            dma((3,)),
            dma((3,)),
            dma((ntp - 1,)),
            dma((ntp - 1,)),
            dma((ntp - 1,)),
            dma((ntp - 1,)),
            dma,
            dma((tokens // WINDOW, 2, longest)),
            dma,
            dma((tokens // WINDOW, 2, longest)),
            dma,
            dma((nsp,)),
            dma,
            dma((chunks, 2, longest)),
            dma,
            dma((chunks + 1, 2, longest)),
            dma,
            dma((nsp,)),
            dma((7,)),
        ],
        compiler_params=pltpu.CompilerParams(collective_id=0, has_side_effects=True),
        name="layer",
    )(
        residual,
        queries,
        keys,
        values,
        meta,
        sinks,
        out_weight,
        norm_gain.reshape(ntp, cols),
        expert_gate,
        expert_up,
        expert_down,
        shared_gate,
        shared_up,
        shared_down,
    )


def solution(mesh):
    in_specs = (
        P(GRP_SP, None),
        P(GRP_SP, "tp"),
        P(GRP_SP, "tp"),
        P(GRP_SP, "tp"),
        P(GRP_SP),
        P(GRP_SP, None),
        P(GRP_SP, None),
        P("tp"),
        P("tp", None),
        P(),
        P("sp", None, "tp"),
        P("sp", None, "tp"),
        P("sp", None, "tp"),
        P(None, "tp"),
        P(None, "tp"),
        P(None, "tp"),
    )
    return jax.shard_map(
        functools.partial(shards, mesh.shape["sp"], mesh.shape["tp"]),
        mesh=mesh,
        in_specs=in_specs,
        out_specs=P(GRP_SP, "tp"),
        check_vma=False,
    )
```

time: 358 us -> 200 us (0.56)
  Pallas kernels: 0 us -> 192 us
  waiting for transfers between devices: 186 us -> 0 us
  blocking collectives: 83.5 us -> 0 us
  starting transfers between devices: 37.3 us -> 0 us
  between operations: 13.8 us -> 0.02 us
  matrix products: 11.9 us -> 0 us
  local copies, waits for them, and re-layouts: 15.8 us -> 4.42 us
  other arithmetic: 8.26 us -> 2.71 us
    pallas_call x0 -> x1, Pallas kernels: none -> 192 us  [shards(): pl.pallas_call(functools.partial(layer, nsp, ntp, cap), out_shape=jax.Sha...]
    all_gather x2 -> x0, waiting for transfers between devices: 107 us -> none  [the longest x1 59.2 us: sent_together(): lax.all_gather(both, axis, axis=dim, tiled=True)]
    all_to_all x3 -> x0, blocking collectives: 72.5 us -> none  [the longest x2 48 us: moved_by_axis(): lax.all_to_all(blocks, axes[k], split_axis=k, concat_axis=k, tiled=True)]
    all_to_all x2 -> x0, waiting for transfers between devices: 52.9 us -> none  [the longest x1 33.1 us: shards(): lax.all_to_all(expert_out.reshape(experts, capacity, col_width), SP, spli...]
    ppermute x3 -> x0, waiting for transfers between devices: 26.1 us -> none  [passed_along(): lax.ppermute(value, axis, [(source, source + steps) for source in range(l...]
    all_to_all x2 -> x0, starting transfers between devices: 22.1 us -> none  [the longest x1 18.3 us: shards(): lax.all_to_all(expert_out.reshape(experts, capacity, col_width), SP, spli...]
    ppermute x3 -> x0, starting transfers between devices: 15.1 us -> none  [passed_along(): lax.ppermute(value, axis, [(source, source + steps) for source in range(l...]
    dot_general x9 -> x0, matrix products: 11.9 us -> none  [the longest x1 3.59 us: shards(): jnp.dot(expert_rows, expert_gate[0], preferred_element_type=jnp.float32)]
  transfers between devices with their start and end apart: 7 -> 0, of which waited for: 6 -> 0; matrix products, arithmetic and copies ran while one was open for 4% -> 0% of each run, Pallas kernels for 0% -> 0%
where the time goes in v1:
time: 200 us; the launch traced here: 199 us
  Pallas kernels  192 us (96%)
  local copies, waits for them, and re-layouts  4.42 us (2%)
  other arithmetic  2.71 us (1%)
    pallas_call x1, Pallas kernels, shards(): pl.pallas_call(functools.partial(layer, nsp, ntp, cap), out_shape=jax.Sha...  192 us

profile of v1, /device:TPU:65, one launch (start us, length us, event | category | flops | bytes accessed | tf_op | source)
XLA Modules:
  0.0 199.2 jit_solution(12838915820531491906)
XLA Ops:
  0.0 0.0 copy-start
  0.0 0.1 pad.3.clone
  0.1 0.7 convert_element_type.12
  0.8 0.7 convert_bitcast_fusion
  1.4 1.3 maximum_maximum_fusion.meta
  2.8 1.3 reshape.4.gain
  4.1 0.0 copy-done
  4.1 0.0 copy-start.1
  4.1 0.7 copy.17.keys
  4.8 0.0 copy-done.1
  4.8 0.7 copy.18.values
  5.6 192.1 %layer.1 = bf16[256,256]{1,0:T(8,128)(2,1)} custom-call(bf16[256,2048]{1,0:T(8,128)(2,1)} %residual.1, bf16[256,128]{1,0:T(8,128)(2,1)} %queries.1, bf16[256,64]{1,0:T(8,128)(2,1)} %copy.17.keys, bf16[256,64]{1,0:T(8,128)(2,1)} %copy.18.values, f32[8,256]{1,0:T(8,128)} %maximum_maximum_fusion.meta, f32[2]{0:T(128)} %sinks.1, bf16[128,2048]{1,0:T(8,128)(2,1)} %out_weight.1, ...), custom_call_target="tpu_custom_call" | custom-call | tf_op jit(solution)/shard_map/layer/pallas_call | solution.py:551
  197.6 1.6 copy.20
  (1 shorter events, 0.0 us)
Async XLA Ops:
  0.0 4.1 %copy-start = (bf16[256,64]{0,1:T(8,128)(2,1)S(1)}, bf16[256,64]{0,1:T(8,128)(2,1)}, u32[]{:S(2)}) copy-start(bf16[256,64]{0,1:T(8,128)(2,1)} %param.18) | copy-start | bytes 98308
  4.1 0.8 copy-start.1

commit v2 on v1

--- a/solution.py
+++ b/solution.py
@@ -17,10 +17,23 @@
 F32 = jnp.float32
 
 
-def delta_order(nz):
-    far = sorted((d if d <= nz // 2 else d - nz for d in range(nz)), key=lambda d: (-abs(d), -d))
-    first = [d for d in far if abs(d) == nz // 4]
-    return first + [d for d in far if d not in first]
+NEAR = 1
+
+
+def source_order(nz):
+    spread = [d if d <= nz // 2 else d - nz for d in range(nz)]
+    far = sorted((d for d in spread if abs(d) > NEAR), key=lambda d: (-abs(d), -d))
+    early = [d for d in far if d == 2] + [d for d in far if abs(d) == 4]
+    far = early + [d for d in far if d not in early]
+    sizes, left = [], len(far)
+    for size in [1] + [2] * len(far):
+        tail = 2 if left > 4 else 1
+        size = min(size, left, tail)
+        if size:
+            sizes.append(size)
+            left -= size
+    near = sorted((d for d in spread if abs(d) <= NEAR), key=lambda d: -abs(d))
+    return far, near, sizes
 
 
 class Ring:
@@ -74,8 +87,8 @@
     def longest(self):
         return self.n // 2
 
-    def finish(self):
-        ref = self.buf.at[pl.ds(0, self.n - 1)]
+    def finish(self, rows):
+        ref = self.buf.at[pl.ds(0, self.n - 1), pl.ds(0, rows)]
         pltpu.make_async_remote_copy(
             src_ref=ref,
             dst_ref=ref,
@@ -94,7 +107,9 @@
     queries,
     keys,
     values,
-    meta,
+    segments,
+    routes,
+    route_weight,
     sinks,
     out_weight,
     gain,
@@ -116,6 +131,8 @@
     scatter,
     pick,
     outgoing,
+    near_out,
+    sums,
     rows_all,
     act_all,
     made,
@@ -134,7 +151,10 @@
     att_recv,
     upd_send,
     upd_recv,
+    sum_send,
+    sum_recv,
     disp_send,
+    near_send,
     disp_recv,
     rows_send,
     rows_recv,
@@ -143,6 +163,7 @@
     ret_send,
     ret_recv,
     load_sem,
+    known_sem,
 ):
     me = lax.axis_index("sp")
     tp = lax.axis_index("tp")
@@ -171,16 +192,35 @@
     for load in loads:
         load.start()
 
+    nearby = [1, 2, -1, -2]
     barrier = pltpu.get_barrier_semaphore()
-    for d in range(1, nsp):
+    for d in nearby:
         pl.semaphore_signal(
-            barrier, inc=1, device_id={"sp": lax.rem(me + d, nsp)}, device_id_type=MESH
+            barrier, inc=1, device_id={"sp": lax.rem(me + d + nsp, nsp)}, device_id_type=MESH
         )
     for d in range(1, ntp):
         pl.semaphore_signal(
             barrier, inc=1, device_id={"tp": lax.rem(tp + d, ntp)}, device_id_type=MESH
         )
-    pl.semaphore_wait(barrier, nsp - 1 + ntp - 1)
+    pl.semaphore_wait(barrier, len(nearby) + ntp - 1)
+    reaches = []
+    while (2 << len(reaches)) < nsp // 2:
+        reaches.append(2 << len(reaches))
+
+    def tell(r):
+        for d in (reaches[r], -reaches[r]):
+            pl.semaphore_signal(
+                known_sem.at[r],
+                inc=1,
+                device_id={"sp": lax.rem(me + d + nsp, nsp)},
+                device_id_type=MESH,
+            )
+
+    def hear(r):
+        pl.semaphore_wait(known_sem.at[r], 2)
+
+    if reaches:
+        tell(0)
 
     tail = pl.ds(tokens - WINDOW, WINDOW)
     halo = [
@@ -193,7 +233,7 @@
             device_id_type=MESH,
         )
         for i, (src, dst) in enumerate(
-            [(keys.at[tail], halo_k), (values.at[tail], halo_v), (meta.at[:, tail], halo_m)]
+            [(keys.at[:, tail], halo_k), (values.at[:, tail], halo_v), (segments.at[:, tail], halo_m)]
         )
     ]
     for copy in halo:
@@ -231,7 +271,8 @@
         )
 
     distances = sorted(range(1, ntp), key=lambda d: min(d, ntp - d))
-    for d in distances:
+    split = len(distances) // 2
+    for d in distances[split:]:
         weight_copy(d).start()
     proj_w[pl.ds(pl.multiple_of(tp * heads_wide, heads_wide), heads_wide), :] = out_weight[
         :, pl.ds(col_start, cols)
@@ -239,8 +280,11 @@
 
     att_ring = Ring(ntp, tp, att, att_send, att_recv)
     upd_ring = Ring(ntp, tp, upd, upd_send, upd_recv)
-    row_meta = meta[...]
-    col_meta = jnp.transpose(row_meta)
+    seg_row = segments[...].astype(F32)
+    weight_row = route_weight[...]
+    col_meta = jnp.transpose(
+        jnp.concatenate([seg_row, weight_row, jnp.zeros((5, tokens), F32)], axis=0)
+    )
     q_pos = lax.broadcasted_iota(jnp.int32, (WINDOW, 2 * WINDOW), 0)
     k_pos = lax.broadcasted_iota(jnp.int32, (WINDOW, 2 * WINDOW), 1)
     offset = q_pos + WINDOW - k_pos
@@ -252,36 +296,44 @@
         heads = []
         for h in range(heads_wide // HEAD_DIM):
             q = queries[rows, h * HEAD_DIM : (h + 1) * HEAD_DIM]
-            scores = lax.dot_general(
-                q, band_k, (((1,), (1,)), ((), ())), preferred_element_type=F32
-            ) * HEAD_DIM ** (-0.5)
+            scores = jnp.dot(q, band_k, preferred_element_type=F32) * HEAD_DIM ** (-0.5)
             masked = jnp.where(allowed, scores, -jnp.inf)
             sink = sinks[h]
             top = jnp.maximum(jnp.max(masked, axis=-1, keepdims=True), sink)
             terms = jnp.exp(masked - top)
             denominator = jnp.sum(terms, axis=-1, keepdims=True) + jnp.exp(sink - top)
             weights = (terms / denominator).astype(BF16)
-            heads.append(jnp.dot(weights, band_v, preferred_element_type=F32).astype(BF16))
+            mixed = lax.dot_general(
+                weights, band_v, (((1,), (1,)), ((), ())), preferred_element_type=F32
+            )
+            heads.append(mixed.astype(BF16))
         att[tp, rows, :] = jnp.concatenate(heads, axis=1)
 
     order = list(range(1, blocks)) + [0]
     span = [pl.ds(b * WINDOW, WINDOW) for b in range(blocks)]
     for b in order[:-1]:
         reach = slice((b - 1) * WINDOW, (b + 1) * WINDOW)
-        attend(b, keys[reach, :], values[reach, :], row_meta[0:1, reach])
+        attend(b, keys[:, reach], values[:, reach], seg_row[:, reach])
         att_ring.begin(span[b], b)
+    for d in distances[:split]:
+        weight_copy(d).start()
+    if reaches:
+        hear(0)
+    if len(reaches) > 1:
+        tell(1)
     for copy in halo:
         copy.wait_recv()
-    halo_seg = jnp.where(me == 0, -1.0, halo_m[0:1, :])
+    first = slice(0, WINDOW)
+    halo_seg = jnp.where(me == 0, -1.0, halo_m[...].astype(F32))
     attend(
         0,
-        jnp.concatenate([halo_k[...], keys[0:WINDOW, :]], axis=0),
-        jnp.concatenate([halo_v[...], values[0:WINDOW, :]], axis=0),
-        jnp.concatenate([halo_seg, row_meta[0:1, 0:WINDOW]], axis=1),
+        jnp.concatenate([halo_k[...], keys[:, first]], axis=1),
+        jnp.concatenate([halo_v[...], values[:, first]], axis=1),
+        jnp.concatenate([halo_seg, seg_row[:, first]], axis=1),
     )
     att_ring.begin(span[0], 0)
 
-    route_of = [row_meta[1 + k : 2 + k, :] for k in range(2)]
+    route_of = [routes[k : k + 1, :].astype(F32) for k in range(2)]
     experts = lax.broadcasted_iota(jnp.int32, (nsp, tokens), 0).astype(F32)
     named = [(experts == r).astype(F32) for r in route_of]
     earlier = lax.broadcasted_iota(jnp.int32, (tokens, tokens), 0)
@@ -309,7 +361,12 @@
         for b in order:
             att_ring.pass_on(span[b], b, hop)
         if hop == 1:
-            for d in distances:
+            for r in range(1, len(reaches)):
+                hear(r)
+                if r + 1 < len(reaches):
+                    tell(r + 1)
+        if hop == 2:
+            for d in distances[split:] + distances[:split]:
                 weight_arrival(d)
     for d in distances:
         pair_copy(d).wait_recv()
@@ -325,22 +382,48 @@
                 preferred_element_type=F32,
             )
         upd[tp, rows, :] = (res[rows, :].astype(F32) + total).astype(BF16)
+    own_cols = upd[tp].astype(F32)
+    squares = jnp.sum(own_cols * own_cols, axis=-1, keepdims=True)
+    sums[tp] = jnp.transpose(jnp.broadcast_to(squares, (tokens, 128)))[0:8, :]
+
+    def sum_copy(d):
+        return pltpu.make_async_remote_copy(
+            src_ref=sums.at[tp],
+            dst_ref=sums.at[tp],
+            send_sem=sum_send.at[d - 1],
+            recv_sem=sum_recv.at[d - 1],
+            device_id={"tp": lax.rem(tp + d, ntp)},
+            device_id_type=MESH,
+        )
+
+    def sum_arrival(d):
+        source = lax.rem(tp - d + ntp, ntp)
+        pltpu.make_async_remote_copy(
+            src_ref=sums.at[source],
+            dst_ref=sums.at[source],
+            send_sem=sum_send.at[d - 1],
+            recv_sem=sum_recv.at[d - 1],
+            device_id={"tp": source},
+            device_id_type=MESH,
+        ).wait_recv()
+
+    for d in distances[::-1]:
+        sum_copy(d).start()
+    for b in order:
         upd_ring.begin(span[b], b)
-    for hop in range(1, upd_ring.longest() + 1):
-        for b in order:
-            upd_ring.pass_on(span[b], b, hop)
-
-    squares = jnp.zeros((tokens, 1), F32)
-    for s in range(ntp):
-        part_rows = upd[s].astype(F32)
-        squares += jnp.sum(part_rows * part_rows, axis=-1, keepdims=True)
-    inv_rms = lax.rsqrt(squares / (ntp * cols) + EPSILON)
-    for s in range(ntp):
-        normed[s] = (upd[s].astype(F32) * inv_rms * gain[s : s + 1, :]).astype(BF16)
-
-    deltas = delta_order(nz)
-    places = [(d, s) for d in deltas for s in range(CORES)]
-    outgoing[...] = jnp.dot(scatter[...], normed[tp], preferred_element_type=F32).astype(BF16)
+    for d in range(1, ntp):
+        sum_arrival(d)
+    squares = sums[0]
+    for s in range(1, ntp):
+        squares += sums[s]
+    inv_rms = jnp.transpose(lax.rsqrt(squares / (ntp * cols) + EPSILON))[:, 0:1]
+
+    far, near, sizes = source_order(nz)
+    places = [(d, s) for d in far + near for s in range(CORES)]
+    far_count = len(far) * CORES
+    own_gain = gain[0:1, pl.ds(col_start, cols)]
+    own_normed = (own_cols * inv_rms * own_gain).astype(BF16)
+    outgoing[...] = jnp.dot(scatter[...], own_normed, preferred_element_type=F32).astype(BF16)
 
     def at_chip(d, s):
         return lax.rem(z + d + nz, nz) * CORES + lax.rem(core + s, CORES)
@@ -360,11 +443,9 @@
             device_id_type=MESH,
         )
 
+    for i in range(far_count):
+        dispatch_copy(i).start()
     own_place = places.index((0, 0))
-    for i in range(nsp):
-        if i != own_place:
-            dispatch_copy(i).start()
-    rows_all[tp, own_place * cap : (own_place + 1) * cap, :] = outgoing[slot_block(me), :]
 
     act_ring = Ring(ntp, tp, act_all, act_send, act_recv)
     rows_ring = Ring(ntp, tp, rows_all, rows_send, rows_recv)
@@ -373,46 +454,94 @@
         gate, up = gate_up[:, :hidden], gate_up[:, hidden:]
         return (gate / (1.0 + jnp.exp(-gate)) * up).astype(BF16)
 
+    starts = [sum(sizes[:q]) * CORES for q in range(len(sizes) + 1)]
+    far_chunks = len(sizes)
+    near_chunk, shared_chunk = far_chunks, far_chunks + 1
+
+    def places_of(q):
+        if q == near_chunk:
+            return range(far_count, nsp)
+        return range(starts[q], starts[q + 1])
+
+    def rows_of(q):
+        if q == shared_chunk:
+            return slots, tokens
+        return places_of(q)[0] * cap, len(places_of(q)) * cap
+
+    def span_of(q):
+        return pl.ds(*rows_of(q))
+
+    def upd_hop(hop):
+        for b in order:
+            upd_ring.pass_on(span[b], b, hop)
+
+    near_places = [i for i in range(far_count, nsp) if i != own_place] + [own_place]
+
+    def near_copy(j):
+        i = near_places[j]
+        target = at_chip(-places[i][0], places[i][1])
+        return pltpu.make_async_remote_copy(
+            src_ref=near_out.at[:, pl.ds(j * cap, cap)],
+            dst_ref=rows_all.at[:, pl.ds(i * cap, cap)],
+            send_sem=near_send,
+            recv_sem=disp_recv.at[i],
+            device_id={"sp": target},
+            device_id_type=MESH,
+        )
+
+    def near_rows():
+        chosen = jnp.concatenate(
+            [scatter[slot_block(at_chip(-places[i][0], places[i][1])), :] for i in near_places],
+            axis=0,
+        )
+        for s in range(ntp):
+            normed[s] = (
+                upd[s].astype(F32) * inv_rms * gain[0:1, s * cols : (s + 1) * cols]
+            ).astype(BF16)
+            picked = jnp.dot(chosen, normed[s], preferred_element_type=F32).astype(BF16)
+            sent = (len(near_places) - 1) * cap
+            near_out[s, 0:sent, :] = picked[:sent]
+            rows_all[s, own_place * cap : (own_place + 1) * cap, :] = picked[sent:]
+        for j in range(len(near_places) - 1):
+            near_copy(j).start()
+
+    def shared_units():
+        total = jnp.zeros((tokens, 2 * hidden), F32)
+        for s in range(ntp):
+            total += jnp.dot(
+                normed[s], shared_in[s * cols : (s + 1) * cols, :], preferred_element_type=F32
+            )
+        act_all[tp, slots : slots + tokens, :] = activate(total)
+        act_ring.begin(span_of(shared_chunk), shared_chunk)
+
     for load in loads[1:]:
         load.wait()
-    total = jnp.zeros((tokens, 2 * hidden), F32)
-    for s in range(ntp):
-        total += jnp.dot(
-            normed[s], shared_in[s * cols : (s + 1) * cols, :], preferred_element_type=F32
-        )
-    act_all[tp, slots : slots + tokens, :] = activate(total)
-    chunk_places = 2 * CORES
-    chunks = nsp // chunk_places
-    chunk = chunk_places * cap
-    shared_span = pl.ds(slots, tokens)
-    act_ring.begin(shared_span, chunks)
 
     def ready(q):
-        for i in range(q * chunk_places, (q + 1) * chunk_places):
-            if i != own_place:
-                dispatch_copy(i).wait_recv()
-        rows_ring.begin(pl.ds(q * chunk, chunk), q)
+        for i in places_of(q):
+            dispatch_copy(i).wait_recv()
+        rows_ring.begin(span_of(q), q)
 
     def rows_hop(q, hop):
-        rows_ring.pass_on(pl.ds(q * chunk, chunk), q, hop)
+        rows_ring.pass_on(span_of(q), q, hop)
 
     def hidden_units(q):
-        rows = slice(q * chunk, (q + 1) * chunk)
-        total = jnp.zeros((chunk, 2 * hidden), F32)
+        if q == near_chunk:
+            for j in range(len(near_places) - 1):
+                near_copy(j).wait_recv()
+        start, count = rows_of(q)
+        total = jnp.zeros((count, 2 * hidden), F32)
         for s in range(ntp):
             total += jnp.dot(
-                rows_all[s, rows, :],
+                rows_all[s, start : start + count, :],
                 expert_in[s * cols : (s + 1) * cols, :],
                 preferred_element_type=F32,
             )
-        act_all[tp, rows, :] = activate(total)
-        act_ring.begin(pl.ds(q * chunk, chunk), q)
+        act_all[tp, start : start + count, :] = activate(total)
+        act_ring.begin(span_of(q), q)
 
     def act_hop(q, hop):
-        act_ring.pass_on(pl.ds(q * chunk, chunk), q, hop)
-
-    def shared_hop(hop):
-        act_ring.pass_on(shared_span, chunks, hop)
+        act_ring.pass_on(span_of(q), q, hop)
 
     def return_copy(i):
         d, s = places[i]
@@ -427,38 +556,52 @@
         )
 
     def outputs(q):
-        rows = slice(q * chunk, (q + 1) * chunk)
-        total = jnp.zeros((chunk, cols), F32)
+        start, count = rows_of(q)
+        total = jnp.zeros((count, cols), F32)
         for s in range(ntp):
             total += jnp.dot(
-                act_all[s, rows, :],
+                act_all[s, start : start + count, :],
                 expert_out[s * hidden : (s + 1) * hidden, :],
                 preferred_element_type=F32,
             )
-        made[rows, :] = total.astype(BF16)
-        for i in range(q * chunk_places, (q + 1) * chunk_places):
+        made[start : start + count, :] = total.astype(BF16)
+        for i in places_of(q):
             if i == own_place:
                 back[slot_block(me), :] = made[i * cap : (i + 1) * cap, :]
             else:
                 return_copy(i).start()
 
-    period, row_hop, act_hop_time = 7.3, 4.0, 3.2
-    head = 4.0
+    row_hop, act_hop_time, upd_hop_time = 5.0, 5.0, 4.0
+    per_distance = 3.7
     longest = rows_ring.longest()
     steps = []
     for hop in range(1, longest + 1):
-        steps.append((hop * 4.0, functools.partial(shared_hop, hop)))
-    for q in range(chunks):
-        at = head + q * period
+        steps.append((hop * upd_hop_time, functools.partial(upd_hop, hop)))
+    steps.append((longest * upd_hop_time + 0.1, functools.partial(near_rows)))
+
+    def act_steps(at, q):
+        for hop in range(1, longest + 1):
+            steps.append((at + hop * act_hop_time, functools.partial(act_hop, q, hop)))
+        at += longest * act_hop_time + 0.1
+        if q != shared_chunk:
+            steps.append((at, functools.partial(outputs, q)))
+
+    at = 4.0
+    for q in range(far_chunks):
         steps.append((at, functools.partial(ready, q)))
         for hop in range(1, longest + 1):
             steps.append((at + hop * row_hop, functools.partial(rows_hop, q, hop)))
-        at += longest * row_hop + 0.1
-        steps.append((at, functools.partial(hidden_units, q)))
-        for hop in range(1, longest + 1):
-            steps.append((at + hop * act_hop_time, functools.partial(act_hop, q, hop)))
-        at += longest * act_hop_time + 0.1
-        steps.append((at, functools.partial(outputs, q)))
+        done = at + longest * row_hop + 0.1
+        steps.append((done, functools.partial(hidden_units, q)))
+        act_steps(done, q)
+        if q + 1 < far_chunks:
+            at += sizes[q] * per_distance
+    at = max(at, longest * upd_hop_time) + 4.0
+    steps.append((at, functools.partial(hidden_units, near_chunk)))
+    act_steps(at, near_chunk)
+    at += 4.0
+    steps.append((at, functools.partial(shared_units)))
+    act_steps(at, shared_chunk)
     for _, step in sorted(steps, key=lambda step: step[0]):
         step()
 
@@ -484,7 +627,7 @@
             ).wait_recv()
     for k in range(2):
         picked = jnp.dot(pick[k], back[...], preferred_element_type=F32)
-        total += picked * col_meta[:, 3 + k : 4 + k]
+        total += picked * col_meta[:, 1 + k : 2 + k]
     out[...] = total.astype(BF16)
 
     for copy in halo:
@@ -492,11 +635,18 @@
     for d in distances:
         weight_copy(d).wait_send()
         pair_copy(d).wait_send()
-    for ring in (att_ring, upd_ring, rows_ring, act_ring):
-        ring.finish()
-    most = pl.ds(0, (nsp - 1) * cap)
-    for buffer, sem in ((outgoing, disp_send), (made, ret_send)):
-        ref = buffer.at[most]
+    for d in range(1, ntp):
+        sum_copy(d).wait_send()
+    att_ring.finish(tokens)
+    upd_ring.finish(tokens)
+    rows_ring.finish(far_count * cap)
+    act_ring.finish(slots + tokens)
+    sent = [
+        (outgoing.at[pl.ds(0, far_count * cap)], disp_send),
+        (near_out, near_send),
+        (made.at[pl.ds(0, (nsp - 1) * cap)], ret_send),
+    ]
+    for ref, sem in sent:
         pltpu.make_async_remote_copy(
             src_ref=ref,
             dst_ref=ref,
@@ -533,17 +683,9 @@
     heads_wide = queries.shape[1]
     cap = 2 * tokens * routes.shape[1] // nsp
     slots = nsp * cap
-    chunks = nsp // (2 * CORES)
     longest = ntp // 2
-    meta = jnp.concatenate(
-        [
-            segments[None].astype(F32),
-            routes.T.astype(F32),
-            route_weight.T,
-            jnp.zeros((3, tokens), F32),
-        ],
-        axis=0,
-    )
+    far, near, sizes = source_order(nsp // CORES)
+    rounds = max(1, (nsp // 4).bit_length() - 1)
     vmem = pl.BlockSpec(memory_space=pltpu.VMEM)
     smem = pl.BlockSpec(memory_space=pltpu.SMEM)
     anywhere = pl.BlockSpec(memory_space=pl.ANY)
@@ -551,12 +693,12 @@
     return pl.pallas_call(
         functools.partial(layer, nsp, ntp, cap),
         out_shape=jax.ShapeDtypeStruct((tokens, cols), BF16),
-        in_specs=[anywhere, vmem, vmem, vmem, vmem, smem, vmem, vmem] + [anywhere] * 6,
+        in_specs=[anywhere] + [vmem] * 6 + [smem, vmem, vmem] + [anywhere] * 6,
         out_specs=vmem,
         scratch_shapes=[
-            pltpu.VMEM((WINDOW, keys.shape[1]), BF16),
-            pltpu.VMEM((WINDOW, values.shape[1]), BF16),
-            pltpu.VMEM((8, WINDOW), F32),
+            pltpu.VMEM((keys.shape[1], WINDOW), BF16),
+            pltpu.VMEM((values.shape[1], WINDOW), BF16),
+            pltpu.VMEM((1, WINDOW), jnp.int32),
             pltpu.VMEM((ntp * heads_wide, cols), BF16),
             pltpu.VMEM((tokens, cols), BF16),
             pltpu.VMEM((ntp, tokens, heads_wide), BF16),
@@ -565,6 +707,8 @@
             pltpu.VMEM((slots, tokens), BF16),
             pltpu.VMEM((2, tokens, slots), BF16),
             pltpu.VMEM((slots, cols), BF16),
+            pltpu.VMEM((ntp, (len(near) * CORES - 1) * cap, cols), BF16),
+            pltpu.VMEM((ntp, 8, tokens), F32),
             pltpu.VMEM((ntp, slots, cols), BF16),
             pltpu.VMEM((ntp, slots + tokens, hidden), BF16),
             pltpu.VMEM((slots, cols), BF16),
@@ -583,27 +727,33 @@
             dma((tokens // WINDOW, 2, longest)),
             dma,
             dma((tokens // WINDOW, 2, longest)),
+            dma((ntp - 1,)),
+            dma((ntp - 1,)),
+            dma,
             dma,
             dma((nsp,)),
             dma,
-            dma((chunks, 2, longest)),
+            dma((len(sizes), 2, longest)),
             dma,
-            dma((chunks + 1, 2, longest)),
+            dma((len(sizes) + 2, 2, longest)),
             dma,
             dma((nsp,)),
             dma((7,)),
+            pltpu.SemaphoreType.REGULAR((rounds,)),
         ],
         compiler_params=pltpu.CompilerParams(collective_id=0, has_side_effects=True),
         name="layer",
     )(
         residual,
         queries,
-        keys,
-        values,
-        meta,
+        keys.T,
+        values.T,
+        segments.reshape(1, tokens),
+        routes.T,
+        route_weight.T,
         sinks,
         out_weight,
-        norm_gain.reshape(ntp, cols),
+        norm_gain.reshape(1, width),
         expert_gate,
         expert_up,
         expert_down,

time: 200 us -> 162 us (0.81)
  Pallas kernels: 192 us -> 161 us
  local copies, waits for them, and re-layouts: 4.42 us -> 1.57 us
  other arithmetic: 2.71 us -> 0 us
    pallas_call x1, Pallas kernels: 192 us -> 161 us  [shards(): pl.pallas_call(functools.partial(layer, nsp, ntp, cap), out_shape=jax.Sha...]
where the time goes in v2:
time: 162 us
  Pallas kernels  161 us (99%)
    pallas_call x1, Pallas kernels, shards(): pl.pallas_call(functools.partial(layer, nsp, ntp, cap), out_shape=jax.Sha...  161 us

profile of v2, /device:TPU:65, one launch (start us, length us, event | category | flops | bytes accessed | tf_op | source)
XLA Modules:
  0.0 162.2 jit_solution(7269973996678370511)
XLA Ops:
  0.0 160.6 %layer.1 = bf16[256,256]{1,0:T(8,128)(2,1)} custom-call(bf16[256,2048]{1,0:T(8,128)(2,1)} %residual.1, bf16[256,128]{1,0:T(8,128)(2,1)} %queries.1, bf16[64,256]{1,0:T(8,128)(2,1)} %bitcast.6, bf16[64,256]{1,0:T(8,128)(2,1)} %bitcast.7, s32[1,256]{1,0:T(1,128)} %bitcast.11, s32[2,256]{1,0:T(2,128)} %bitcast.9, f32[2,256]{1,0:T(2,128)} %bitcast.10, f32[2]{0:T(128)} %sinks.1, ...), custom_call_target="tpu_custom_call" | custom-call | tf_op jit(solution)/shard_map/layer/pallas_call | solution.py:693
  160.6 1.6 copy.18

commit v3 on v2

--- a/solution.py
+++ b/solution.py
@@ -17,23 +17,17 @@
 F32 = jnp.float32
 
 
-NEAR = 1
-
-
-def source_order(nz):
+def send_order(nz):
     spread = [d if d <= nz // 2 else d - nz for d in range(nz)]
-    far = sorted((d for d in spread if abs(d) > NEAR), key=lambda d: (-abs(d), -d))
-    early = [d for d in far if d == 2] + [d for d in far if abs(d) == 4]
-    far = early + [d for d in far if d not in early]
-    sizes, left = [], len(far)
-    for size in [1] + [2] * len(far):
-        tail = 2 if left > 4 else 1
-        size = min(size, left, tail)
-        if size:
-            sizes.append(size)
-            left -= size
-    near = sorted((d for d in spread if abs(d) <= NEAR), key=lambda d: -abs(d))
-    return far, near, sizes
+    by_reach = sorted(spread, key=lambda d: (abs(d), -d))
+    order = []
+    while by_reach:
+        order.append(by_reach.pop(0))
+        if by_reach:
+            order.append(by_reach.pop(0))
+        if by_reach:
+            order.append(by_reach.pop())
+    return order
 
 
 class Ring:
@@ -97,6 +91,38 @@
             device_id={"tp": self.me},
             device_id_type=MESH,
         ).wait_send()
+
+
+class Leaps(Ring):
+    def copy(self, rows, index, right, hop):
+        step = 1 if right else -1
+        kept = 0 if hop <= 2 else 2
+        origin = lax.rem(self.me - step * kept + self.n, self.n)
+        target = lax.rem(self.me + step * (hop - kept) + self.n, self.n)
+        ref = self.buf.at[origin, rows]
+        return pltpu.make_async_remote_copy(
+            src_ref=ref,
+            dst_ref=ref,
+            send_sem=self.send_sem,
+            recv_sem=self.recv_sem.at[index, 0 if right else 1, hop - 1],
+            device_id={"tp": target},
+            device_id_type=MESH,
+        )
+
+    def begin(self, rows, index):
+        for hop in (2, 1):
+            for right in (True, False):
+                if hop <= self.hops(index, right):
+                    self.copy(rows, index, right, hop).start()
+
+    def pass_on(self, rows, index, hop):
+        for right in (True, False):
+            most = self.hops(index, right)
+            if hop <= most:
+                self.arrival(rows, index, right, hop)
+                if hop == 2:
+                    for later in range(most, 2, -1):
+                        self.copy(rows, index, right, later).start()
 
 
 def layer(
@@ -131,7 +157,6 @@
     scatter,
     pick,
     outgoing,
-    near_out,
     sums,
     rows_all,
     act_all,
@@ -154,7 +179,6 @@
     sum_send,
     sum_recv,
     disp_send,
-    near_send,
     disp_recv,
     rows_send,
     rows_recv,
@@ -163,7 +187,8 @@
     ret_send,
     ret_recv,
     load_sem,
-    known_sem,
+    chain_sem,
+    all_in,
 ):
     me = lax.axis_index("sp")
     tp = lax.axis_index("tp")
@@ -192,35 +217,37 @@
     for load in loads:
         load.start()
 
-    nearby = [1, 2, -1, -2]
+    def say(semaphore, where):
+        pl.semaphore_signal(semaphore, inc=1, device_id=where, device_id_type=MESH)
+
+    last = (me + 1) // nsp
     barrier = pltpu.get_barrier_semaphore()
-    for d in nearby:
-        pl.semaphore_signal(
-            barrier, inc=1, device_id={"sp": lax.rem(me + d + nsp, nsp)}, device_id_type=MESH
-        )
     for d in range(1, ntp):
-        pl.semaphore_signal(
-            barrier, inc=1, device_id={"tp": lax.rem(tp + d, ntp)}, device_id_type=MESH
-        )
-    pl.semaphore_wait(barrier, len(nearby) + ntp - 1)
-    reaches = []
-    while (2 << len(reaches)) < nsp // 2:
-        reaches.append(2 << len(reaches))
-
-    def tell(r):
-        for d in (reaches[r], -reaches[r]):
-            pl.semaphore_signal(
-                known_sem.at[r],
-                inc=1,
-                device_id={"sp": lax.rem(me + d + nsp, nsp)},
-                device_id_type=MESH,
-            )
-
-    def hear(r):
-        pl.semaphore_wait(known_sem.at[r], 2)
-
-    if reaches:
-        tell(0)
+        say(barrier, {"tp": lax.rem(tp + d, ntp)})
+    say(barrier, {"sp": sibling})
+
+    @pl.when(core == 0)
+    def _():
+        say(barrier, {"sp": lax.rem(me + nsp - 1, nsp)})
+
+    @pl.when(me == 1)
+    def _():
+        say(barrier, {"sp": nsp - 1})
+
+    pl.semaphore_wait(barrier, ntp + core + last)
+
+    @pl.when(me >= 3)
+    def _():
+        pl.semaphore_wait(chain_sem, 1)
+
+    @pl.when((me >= 2) & (me < nsp - 1))
+    def _():
+        say(chain_sem, {"sp": following})
+
+    @pl.when(me == nsp - 1)
+    def _():
+        for j in range(nsp - 1):
+            say(all_in, {"sp": j})
 
     tail = pl.ds(tokens - WINDOW, WINDOW)
     halo = [
@@ -236,8 +263,12 @@
             [(keys.at[:, tail], halo_k), (values.at[:, tail], halo_v), (segments.at[:, tail], halo_m)]
         )
     ]
-    for copy in halo:
-        copy.start()
+
+    @pl.when(me < nsp - 1)
+    def _():
+        for copy in halo:
+            copy.start()
+
 
     part = heads_wide // CORES
 
@@ -278,7 +309,7 @@
         :, pl.ds(col_start, cols)
     ]
 
-    att_ring = Ring(ntp, tp, att, att_send, att_recv)
+    att_ring = Leaps(ntp, tp, att, att_send, att_recv)
     upd_ring = Ring(ntp, tp, upd, upd_send, upd_recv)
     seg_row = segments[...].astype(F32)
     weight_row = route_weight[...]
@@ -317,12 +348,17 @@
         att_ring.begin(span[b], b)
     for d in distances[:split]:
         weight_copy(d).start()
-    if reaches:
-        hear(0)
-    if len(reaches) > 1:
-        tell(1)
-    for copy in halo:
-        copy.wait_recv()
+
+    @pl.when(me > 0)
+    def _():
+        for copy in halo:
+            copy.wait_recv()
+
+    @pl.when(me == 0)
+    def _():
+        for ref in (halo_k, halo_v, halo_m):
+            ref[...] = jnp.zeros_like(ref)
+
     first = slice(0, WINDOW)
     halo_seg = jnp.where(me == 0, -1.0, halo_m[...].astype(F32))
     attend(
@@ -357,15 +393,11 @@
         weight_copy(d).wait_recv()
         pair_copy(d).start()
 
-    for hop in range(1, att_ring.longest() + 1):
+    hops = list(range(1, att_ring.longest() + 1))
+    for hop in hops[1:2] + hops[:1] + hops[2:]:
         for b in order:
             att_ring.pass_on(span[b], b, hop)
         if hop == 1:
-            for r in range(1, len(reaches)):
-                hear(r)
-                if r + 1 < len(reaches):
-                    tell(r + 1)
-        if hop == 2:
             for d in distances[split:] + distances[:split]:
                 weight_arrival(d)
     for d in distances:
@@ -418,9 +450,8 @@
         squares += sums[s]
     inv_rms = jnp.transpose(lax.rsqrt(squares / (ntp * cols) + EPSILON))[:, 0:1]
 
-    far, near, sizes = source_order(nz)
-    places = [(d, s) for d in far + near for s in range(CORES)]
-    far_count = len(far) * CORES
+    chips = send_order(nz)
+    places = [(d, s) for d in chips for s in range(CORES) if (d, s) != (0, 0)]
     own_gain = gain[0:1, pl.ds(col_start, cols)]
     own_normed = (own_cols * inv_rms * own_gain).astype(BF16)
     outgoing[...] = jnp.dot(scatter[...], own_normed, preferred_element_type=F32).astype(BF16)
@@ -433,19 +464,34 @@
 
     def dispatch_copy(i):
         d, s = places[i]
-        target = at_chip(-d, s)
+        target = at_chip(d, s)
         return pltpu.make_async_remote_copy(
             src_ref=outgoing.at[slot_block(target)],
-            dst_ref=rows_all.at[tp, pl.ds(i * cap, cap)],
+            dst_ref=rows_all.at[tp, slot_block(me)],
             send_sem=disp_send,
-            recv_sem=disp_recv.at[i],
+            recv_sem=disp_recv.at[me],
             device_id={"sp": target},
             device_id_type=MESH,
         )
 
-    for i in range(far_count):
+    rows_all[tp, slot_block(me), :] = outgoing[slot_block(me), :]
+
+    @pl.when(me < nsp - 1)
+    def _():
+        pl.semaphore_wait(all_in, 1)
+
+    for i in range(len(places)):
         dispatch_copy(i).start()
-    own_place = places.index((0, 0))
+
+    def block_wait(ref, sem):
+        pltpu.make_async_remote_copy(
+            src_ref=ref,
+            dst_ref=ref,
+            send_sem=disp_send,
+            recv_sem=sem,
+            device_id={"sp": me},
+            device_id_type=MESH,
+        ).wait_recv()
 
     act_ring = Ring(ntp, tp, act_all, act_send, act_recv)
     rows_ring = Ring(ntp, tp, rows_all, rows_send, rows_recv)
@@ -454,19 +500,17 @@
         gate, up = gate_up[:, :hidden], gate_up[:, hidden:]
         return (gate / (1.0 + jnp.exp(-gate)) * up).astype(BF16)
 
-    starts = [sum(sizes[:q]) * CORES for q in range(len(sizes) + 1)]
-    far_chunks = len(sizes)
-    near_chunk, shared_chunk = far_chunks, far_chunks + 1
+    chunk_sources = 2 * CORES
+    chunks = nsp // chunk_sources
+    shared_chunk = chunks
 
     def places_of(q):
-        if q == near_chunk:
-            return range(far_count, nsp)
-        return range(starts[q], starts[q + 1])
+        return range(q * chunk_sources, (q + 1) * chunk_sources)
 
     def rows_of(q):
         if q == shared_chunk:
             return slots, tokens
-        return places_of(q)[0] * cap, len(places_of(q)) * cap
+        return q * chunk_sources * cap, chunk_sources * cap
 
     def span_of(q):
         return pl.ds(*rows_of(q))
@@ -475,39 +519,12 @@
         for b in order:
             upd_ring.pass_on(span[b], b, hop)
 
-    near_places = [i for i in range(far_count, nsp) if i != own_place] + [own_place]
-
-    def near_copy(j):
-        i = near_places[j]
-        target = at_chip(-places[i][0], places[i][1])
-        return pltpu.make_async_remote_copy(
-            src_ref=near_out.at[:, pl.ds(j * cap, cap)],
-            dst_ref=rows_all.at[:, pl.ds(i * cap, cap)],
-            send_sem=near_send,
-            recv_sem=disp_recv.at[i],
-            device_id={"sp": target},
-            device_id_type=MESH,
-        )
-
-    def near_rows():
-        chosen = jnp.concatenate(
-            [scatter[slot_block(at_chip(-places[i][0], places[i][1])), :] for i in near_places],
-            axis=0,
-        )
+    def shared_units():
+        total = jnp.zeros((tokens, 2 * hidden), F32)
         for s in range(ntp):
             normed[s] = (
                 upd[s].astype(F32) * inv_rms * gain[0:1, s * cols : (s + 1) * cols]
             ).astype(BF16)
-            picked = jnp.dot(chosen, normed[s], preferred_element_type=F32).astype(BF16)
-            sent = (len(near_places) - 1) * cap
-            near_out[s, 0:sent, :] = picked[:sent]
-            rows_all[s, own_place * cap : (own_place + 1) * cap, :] = picked[sent:]
-        for j in range(len(near_places) - 1):
-            near_copy(j).start()
-
-    def shared_units():
-        total = jnp.zeros((tokens, 2 * hidden), F32)
-        for s in range(ntp):
             total += jnp.dot(
                 normed[s], shared_in[s * cols : (s + 1) * cols, :], preferred_element_type=F32
             )
@@ -518,17 +535,18 @@
         load.wait()
 
     def ready(q):
-        for i in places_of(q):
-            dispatch_copy(i).wait_recv()
+        for source in places_of(q):
+
+            @pl.when(me != source)
+            def _():
+                block_wait(rows_all.at[tp, pl.ds(source * cap, cap)], disp_recv.at[source])
+
         rows_ring.begin(span_of(q), q)
 
     def rows_hop(q, hop):
         rows_ring.pass_on(span_of(q), q, hop)
 
     def hidden_units(q):
-        if q == near_chunk:
-            for j in range(len(near_places) - 1):
-                near_copy(j).wait_recv()
         start, count = rows_of(q)
         total = jnp.zeros((count, 2 * hidden), F32)
         for s in range(ntp):
@@ -543,15 +561,13 @@
     def act_hop(q, hop):
         act_ring.pass_on(span_of(q), q, hop)
 
-    def return_copy(i):
-        d, s = places[i]
-        target = at_chip(d, s)
+    def return_copy(source):
         return pltpu.make_async_remote_copy(
-            src_ref=made.at[pl.ds(i * cap, cap)],
+            src_ref=made.at[pl.ds(source * cap, cap)],
             dst_ref=back.at[slot_block(me)],
             send_sem=ret_send,
-            recv_sem=ret_recv.at[i],
-            device_id={"sp": target},
+            recv_sem=ret_recv.at[me],
+            device_id={"sp": source},
             device_id_type=MESH,
         )
 
@@ -565,19 +581,21 @@
                 preferred_element_type=F32,
             )
         made[start : start + count, :] = total.astype(BF16)
-        for i in places_of(q):
-            if i == own_place:
-                back[slot_block(me), :] = made[i * cap : (i + 1) * cap, :]
-            else:
-                return_copy(i).start()
-
-    row_hop, act_hop_time, upd_hop_time = 5.0, 5.0, 4.0
-    per_distance = 3.7
+        for source in places_of(q):
+
+            @pl.when(me == source)
+            def _():
+                back[slot_block(me), :] = made[source * cap : (source + 1) * cap, :]
+
+            @pl.when(me != source)
+            def _():
+                return_copy(source).start()
+
+    row_hop, act_hop_time, upd_hop_time, period = 5.0, 5.0, 3.0, 7.4
     longest = rows_ring.longest()
     steps = []
     for hop in range(1, longest + 1):
         steps.append((hop * upd_hop_time, functools.partial(upd_hop, hop)))
-    steps.append((longest * upd_hop_time + 0.1, functools.partial(near_rows)))
 
     def act_steps(at, q):
         for hop in range(1, longest + 1):
@@ -586,20 +604,17 @@
         if q != shared_chunk:
             steps.append((at, functools.partial(outputs, q)))
 
-    at = 4.0
-    for q in range(far_chunks):
+    in_turn = list(range(1, min(3, chunks))) + [0] + list(range(3, chunks))
+    at = 8.0
+    for q in in_turn:
         steps.append((at, functools.partial(ready, q)))
         for hop in range(1, longest + 1):
             steps.append((at + hop * row_hop, functools.partial(rows_hop, q, hop)))
         done = at + longest * row_hop + 0.1
         steps.append((done, functools.partial(hidden_units, q)))
         act_steps(done, q)
-        if q + 1 < far_chunks:
-            at += sizes[q] * per_distance
-    at = max(at, longest * upd_hop_time) + 4.0
-    steps.append((at, functools.partial(hidden_units, near_chunk)))
-    act_steps(at, near_chunk)
-    at += 4.0
+        at += period
+    at = max(at, longest * upd_hop_time) + 1.0
     steps.append((at, functools.partial(shared_units)))
     act_steps(at, shared_chunk)
     for _, step in sorted(steps, key=lambda step: step[0]):
@@ -612,26 +627,22 @@
             shared_out[s * hidden : (s + 1) * hidden, :],
             preferred_element_type=F32,
         )
-    for i in range(nsp):
-        if i != own_place:
-            d, s = places[i]
-            source = at_chip(-d, s)
-            ref = back.at[slot_block(source)]
-            pltpu.make_async_remote_copy(
-                src_ref=ref,
-                dst_ref=ref,
-                send_sem=ret_send,
-                recv_sem=ret_recv.at[i],
-                device_id={"sp": source},
-                device_id_type=MESH,
-            ).wait_recv()
+    for expert in range(nsp):
+
+        @pl.when(me != expert)
+        def _():
+            block_wait(back.at[pl.ds(expert * cap, cap)], ret_recv.at[expert])
+
     for k in range(2):
         picked = jnp.dot(pick[k], back[...], preferred_element_type=F32)
         total += picked * col_meta[:, 1 + k : 2 + k]
     out[...] = total.astype(BF16)
 
-    for copy in halo:
-        copy.wait_send()
+    @pl.when(me < nsp - 1)
+    def _():
+        for copy in halo:
+            copy.wait_send()
+
     for d in distances:
         weight_copy(d).wait_send()
         pair_copy(d).wait_send()
@@ -639,11 +650,10 @@
         sum_copy(d).wait_send()
     att_ring.finish(tokens)
     upd_ring.finish(tokens)
-    rows_ring.finish(far_count * cap)
+    rows_ring.finish(slots)
     act_ring.finish(slots + tokens)
     sent = [
-        (outgoing.at[pl.ds(0, far_count * cap)], disp_send),
-        (near_out, near_send),
+        (outgoing.at[pl.ds(0, (nsp - 1) * cap)], disp_send),
         (made.at[pl.ds(0, (nsp - 1) * cap)], ret_send),
     ]
     for ref, sem in sent:
@@ -684,8 +694,7 @@
     cap = 2 * tokens * routes.shape[1] // nsp
     slots = nsp * cap
     longest = ntp // 2
-    far, near, sizes = source_order(nsp // CORES)
-    rounds = max(1, (nsp // 4).bit_length() - 1)
+    chunks = nsp // (2 * CORES)
     vmem = pl.BlockSpec(memory_space=pltpu.VMEM)
     smem = pl.BlockSpec(memory_space=pltpu.SMEM)
     anywhere = pl.BlockSpec(memory_space=pl.ANY)
@@ -707,7 +716,6 @@
             pltpu.VMEM((slots, tokens), BF16),
             pltpu.VMEM((2, tokens, slots), BF16),
             pltpu.VMEM((slots, cols), BF16),
-            pltpu.VMEM((ntp, (len(near) * CORES - 1) * cap, cols), BF16),
             pltpu.VMEM((ntp, 8, tokens), F32),
             pltpu.VMEM((ntp, slots, cols), BF16),
             pltpu.VMEM((ntp, slots + tokens, hidden), BF16),
@@ -730,16 +738,16 @@
             dma((ntp - 1,)),
             dma((ntp - 1,)),
             dma,
-            dma,
             dma((nsp,)),
             dma,
-            dma((len(sizes), 2, longest)),
+            dma((chunks, 2, longest)),
             dma,
-            dma((len(sizes) + 2, 2, longest)),
+            dma((chunks + 1, 2, longest)),
             dma,
             dma((nsp,)),
             dma((7,)),
-            pltpu.SemaphoreType.REGULAR((rounds,)),
+            pltpu.SemaphoreType.REGULAR,
+            pltpu.SemaphoreType.REGULAR,
         ],
         compiler_params=pltpu.CompilerParams(collective_id=0, has_side_effects=True),
         name="layer",

time: 162 us -> 163 us (level)
  no operation moved by 1% of the time
where the time goes in v3:
time: 163 us; the launch traced here: 162 us
  Pallas kernels  161 us (99%)
    pallas_call x1, Pallas kernels, shards(): pl.pallas_call(functools.partial(layer, nsp, ntp, cap), out_shape=jax.Sha...  161 us

profile of v3, /device:TPU:65, one launch (start us, length us, event | category | flops | bytes accessed | tf_op | source)
XLA Modules:
  0.0 162.4 jit_solution(14136617558086691437)
XLA Ops:
  0.0 160.8 %layer.1 = bf16[256,256]{1,0:T(8,128)(2,1)} custom-call(bf16[256,2048]{1,0:T(8,128)(2,1)} %residual.1, bf16[256,128]{1,0:T(8,128)(2,1)} %queries.1, bf16[64,256]{1,0:T(8,128)(2,1)} %bitcast.6, bf16[64,256]{1,0:T(8,128)(2,1)} %bitcast.7, s32[1,256]{1,0:T(1,128)} %bitcast.11, s32[2,256]{1,0:T(2,128)} %bitcast.9, f32[2,256]{1,0:T(2,128)} %bitcast.10, f32[2]{0:T(128)} %sinks.1, ...), custom_call_target="tpu_custom_call" | custom-call | tf_op jit(solution)/shard_map/layer/pallas_call | solution.py:702
  160.8 1.6 copy.18

commit v4 on v3

--- a/solution.py
+++ b/solution.py
@@ -157,6 +157,7 @@
     scatter,
     pick,
     outgoing,
+    near_out,
     sums,
     rows_all,
     act_all,
@@ -179,6 +180,7 @@
     sum_send,
     sum_recv,
     disp_send,
+    near_send,
     disp_recv,
     rows_send,
     rows_recv,
@@ -246,7 +248,8 @@
 
     @pl.when(me == nsp - 1)
     def _():
-        for j in range(nsp - 1):
+        reach = [min(j // CORES + 1, nz - 1 - j // CORES) for j in range(nsp - 1)]
+        for j in sorted(range(nsp - 1), key=lambda j: -reach[j]):
             say(all_in, {"sp": j})
 
     tail = pl.ds(tokens - WINDOW, WINDOW)
@@ -474,14 +477,21 @@
             device_id_type=MESH,
         )
 
-    rows_all[tp, slot_block(me), :] = outgoing[slot_block(me), :]
+    chunk_sources = 2 * CORES
+    chunks = nsp // chunk_sources
+    own_chunk = me // chunk_sources
 
     @pl.when(me < nsp - 1)
     def _():
         pl.semaphore_wait(all_in, 1)
 
     for i in range(len(places)):
-        dispatch_copy(i).start()
+        far = at_chip(*places[i]) // chunk_sources != own_chunk
+
+        @pl.when(far)
+        def _():
+            dispatch_copy(i).start()
+
 
     def block_wait(ref, sem):
         pltpu.make_async_remote_copy(
@@ -500,9 +510,35 @@
         gate, up = gate_up[:, :hidden], gate_up[:, hidden:]
         return (gate / (1.0 + jnp.exp(-gate)) * up).astype(BF16)
 
-    chunk_sources = 2 * CORES
-    chunks = nsp // chunk_sources
     shared_chunk = chunks
+    partners = [
+        own_chunk * chunk_sources + lax.rem(me + k, chunk_sources) for k in range(1, chunk_sources)
+    ]
+
+    def near_copy(k):
+        return pltpu.make_async_remote_copy(
+            src_ref=near_out.at[:, pl.ds(k * cap, cap)],
+            dst_ref=rows_all.at[:, slot_block(me)],
+            send_sem=near_send,
+            recv_sem=disp_recv.at[me],
+            device_id={"sp": partners[k]},
+            device_id_type=MESH,
+        )
+
+    def near_rows():
+        chosen = jnp.concatenate(
+            [scatter[slot_block(target), :] for target in partners + [me]], axis=0
+        )
+        sent = len(partners) * cap
+        for s in range(ntp):
+            normed[s] = (
+                upd[s].astype(F32) * inv_rms * gain[0:1, s * cols : (s + 1) * cols]
+            ).astype(BF16)
+            picked = jnp.dot(chosen, normed[s], preferred_element_type=F32).astype(BF16)
+            near_out[s, :, :] = picked[:sent]
+            rows_all[s, slot_block(me), :] = picked[sent:]
+        for k in range(len(partners)):
+            near_copy(k).start()
 
     def places_of(q):
         return range(q * chunk_sources, (q + 1) * chunk_sources)
@@ -522,9 +558,6 @@
     def shared_units():
         total = jnp.zeros((tokens, 2 * hidden), F32)
         for s in range(ntp):
-            normed[s] = (
-                upd[s].astype(F32) * inv_rms * gain[0:1, s * cols : (s + 1) * cols]
-            ).astype(BF16)
             total += jnp.dot(
                 normed[s], shared_in[s * cols : (s + 1) * cols, :], preferred_element_type=F32
             )
@@ -535,18 +568,23 @@
         load.wait()
 
     def ready(q):
-        for source in places_of(q):
-
-            @pl.when(me != source)
-            def _():
+        @pl.when(own_chunk != q)
+        def _():
+            for source in places_of(q):
                 block_wait(rows_all.at[tp, pl.ds(source * cap, cap)], disp_recv.at[source])
-
-        rows_ring.begin(span_of(q), q)
+            rows_ring.begin(span_of(q), q)
 
     def rows_hop(q, hop):
-        rows_ring.pass_on(span_of(q), q, hop)
+        @pl.when(own_chunk != q)
+        def _():
+            rows_ring.pass_on(span_of(q), q, hop)
 
     def hidden_units(q):
+        @pl.when(own_chunk == q)
+        def _():
+            for source in partners:
+                block_wait(rows_all.at[:, slot_block(source)], disp_recv.at[source])
+
         start, count = rows_of(q)
         total = jnp.zeros((count, 2 * hidden), F32)
         for s in range(ntp):
@@ -597,6 +635,8 @@
     for hop in range(1, longest + 1):
         steps.append((hop * upd_hop_time, functools.partial(upd_hop, hop)))
 
+    steps.append((longest * upd_hop_time + 0.1, functools.partial(near_rows)))
+
     def act_steps(at, q):
         for hop in range(1, longest + 1):
             steps.append((at + hop * act_hop_time, functools.partial(act_hop, q, hop)))
@@ -614,7 +654,7 @@
         steps.append((done, functools.partial(hidden_units, q)))
         act_steps(done, q)
         at += period
-    at = max(at, longest * upd_hop_time) + 1.0
+    at = max(at, longest * upd_hop_time) + 13.0
     steps.append((at, functools.partial(shared_units)))
     act_steps(at, shared_chunk)
     for _, step in sorted(steps, key=lambda step: step[0]):
@@ -650,10 +690,11 @@
         sum_copy(d).wait_send()
     att_ring.finish(tokens)
     upd_ring.finish(tokens)
-    rows_ring.finish(slots)
+    rows_ring.finish((nsp - chunk_sources) * cap)
     act_ring.finish(slots + tokens)
     sent = [
-        (outgoing.at[pl.ds(0, (nsp - 1) * cap)], disp_send),
+        (outgoing.at[pl.ds(0, (nsp - chunk_sources) * cap)], disp_send),
+        (near_out, near_send),
         (made.at[pl.ds(0, (nsp - 1) * cap)], ret_send),
     ]
     for ref, sem in sent:
@@ -716,6 +757,7 @@
             pltpu.VMEM((slots, tokens), BF16),
             pltpu.VMEM((2, tokens, slots), BF16),
             pltpu.VMEM((slots, cols), BF16),
+            pltpu.VMEM((ntp, (2 * CORES - 1) * cap, cols), BF16),
             pltpu.VMEM((ntp, 8, tokens), F32),
             pltpu.VMEM((ntp, slots, cols), BF16),
             pltpu.VMEM((ntp, slots + tokens, hidden), BF16),
@@ -737,6 +779,7 @@
             dma((tokens // WINDOW, 2, longest)),
             dma((ntp - 1,)),
             dma((ntp - 1,)),
+            dma,
             dma,
             dma((nsp,)),
             dma,

time: 163 us -> 157 us (0.963)
  Pallas kernels: 161 us -> 155 us
    pallas_call x1, Pallas kernels: 161 us -> 155 us  [shards(): pl.pallas_call(functools.partial(layer, nsp, ntp, cap), out_shape=jax.Sha...]
where the time goes in v4:
time: 157 us
  Pallas kernels  155 us (99%)
  local copies, waits for them, and re-layouts  1.57 us (1%)
    pallas_call x1, Pallas kernels, shards(): pl.pallas_call(functools.partial(layer, nsp, ntp, cap), out_shape=jax.Sha...  155 us

profile of v4, /device:TPU:65, one launch (start us, length us, event | category | flops | bytes accessed | tf_op | source)
XLA Modules:
  0.0 157.0 jit_solution(3732814024619060290)
XLA Ops:
  0.0 155.4 %layer.1 = bf16[256,256]{1,0:T(8,128)(2,1)} custom-call(bf16[256,2048]{1,0:T(8,128)(2,1)} %residual.1, bf16[256,128]{1,0:T(8,128)(2,1)} %queries.1, bf16[64,256]{1,0:T(8,128)(2,1)} %bitcast.6, bf16[64,256]{1,0:T(8,128)(2,1)} %bitcast.7, s32[1,256]{1,0:T(1,128)} %bitcast.11, s32[2,256]{1,0:T(2,128)} %bitcast.9, f32[2,256]{1,0:T(2,128)} %bitcast.10, f32[2]{0:T(128)} %sinks.1, ...), custom_call_target="tpu_custom_call" | custom-call | tf_op jit(solution)/shard_map/layer/pallas_call | solution.py:743
  155.4 1.6 copy.18

commit v5 on v4

--- a/solution.py
+++ b/solution.py
@@ -540,13 +540,20 @@
         for k in range(len(partners)):
             near_copy(k).start()
 
+    half = me // (nsp // 2)
+
+    def taken(q):
+        if q == chunks - 2:
+            return q + half
+        return q - half if q == chunks - 1 else q
+
     def places_of(q):
-        return range(q * chunk_sources, (q + 1) * chunk_sources)
+        return [taken(q) * chunk_sources + k for k in range(chunk_sources)]
 
     def rows_of(q):
         if q == shared_chunk:
             return slots, tokens
-        return q * chunk_sources * cap, chunk_sources * cap
+        return pl.multiple_of(taken(q) * chunk_sources * cap, cap), chunk_sources * cap
 
     def span_of(q):
         return pl.ds(*rows_of(q))
@@ -568,19 +575,19 @@
         load.wait()
 
     def ready(q):
-        @pl.when(own_chunk != q)
+        @pl.when(own_chunk != taken(q))
         def _():
             for source in places_of(q):
-                block_wait(rows_all.at[tp, pl.ds(source * cap, cap)], disp_recv.at[source])
+                block_wait(rows_all.at[tp, slot_block(source)], disp_recv.at[source])
             rows_ring.begin(span_of(q), q)
 
     def rows_hop(q, hop):
-        @pl.when(own_chunk != q)
+        @pl.when(own_chunk != taken(q))
         def _():
             rows_ring.pass_on(span_of(q), q, hop)
 
     def hidden_units(q):
-        @pl.when(own_chunk == q)
+        @pl.when(own_chunk == taken(q))
         def _():
             for source in partners:
                 block_wait(rows_all.at[:, slot_block(source)], disp_recv.at[source])
@@ -589,11 +596,11 @@
         total = jnp.zeros((count, 2 * hidden), F32)
         for s in range(ntp):
             total += jnp.dot(
-                rows_all[s, start : start + count, :],
+                rows_all[s, pl.ds(start, count), :],
                 expert_in[s * cols : (s + 1) * cols, :],
                 preferred_element_type=F32,
             )
-        act_all[tp, start : start + count, :] = activate(total)
+        act_all[tp, pl.ds(start, count), :] = activate(total)
         act_ring.begin(span_of(q), q)
 
     def act_hop(q, hop):
@@ -601,7 +608,7 @@
 
     def return_copy(source):
         return pltpu.make_async_remote_copy(
-            src_ref=made.at[pl.ds(source * cap, cap)],
+            src_ref=made.at[slot_block(source)],
             dst_ref=back.at[slot_block(me)],
             send_sem=ret_send,
             recv_sem=ret_recv.at[me],
@@ -614,16 +621,16 @@
         total = jnp.zeros((count, cols), F32)
         for s in range(ntp):
             total += jnp.dot(
-                act_all[s, start : start + count, :],
+                act_all[s, pl.ds(start, count), :],
                 expert_out[s * hidden : (s + 1) * hidden, :],
                 preferred_element_type=F32,
             )
-        made[start : start + count, :] = total.astype(BF16)
+        made[pl.ds(start, count), :] = total.astype(BF16)
         for source in places_of(q):
 
             @pl.when(me == source)
             def _():
-                back[slot_block(me), :] = made[source * cap : (source + 1) * cap, :]
+                back[slot_block(me), :] = made[slot_block(source), :]
 
             @pl.when(me != source)
             def _():
@@ -645,7 +652,7 @@
             steps.append((at, functools.partial(outputs, q)))
 
     in_turn = list(range(1, min(3, chunks))) + [0] + list(range(3, chunks))
-    at = 8.0
+    at = 9.5
     for q in in_turn:
         steps.append((at, functools.partial(ready, q)))
         for hop in range(1, longest + 1):

time: 157 us -> 158 us (level)
  no operation moved by 1% of the time
where the time goes in v5:
time: 158 us; the launch traced here: 157 us
  Pallas kernels  155 us (98%)
    pallas_call x1, Pallas kernels, shards(): pl.pallas_call(functools.partial(layer, nsp, ntp, cap), out_shape=jax.Sha...  155 us

profile of v5, /device:TPU:65, one launch (start us, length us, event | category | flops | bytes accessed | tf_op | source)
XLA Modules:
  0.0 156.5 jit_solution(3729915990252023994)
XLA Ops:
  0.0 154.9 %layer.1 = bf16[256,256]{1,0:T(8,128)(2,1)} custom-call(bf16[256,2048]{1,0:T(8,128)(2,1)} %residual.1, bf16[256,128]{1,0:T(8,128)(2,1)} %queries.1, bf16[64,256]{1,0:T(8,128)(2,1)} %bitcast.6, bf16[64,256]{1,0:T(8,128)(2,1)} %bitcast.7, s32[1,256]{1,0:T(1,128)} %bitcast.11, s32[2,256]{1,0:T(2,128)} %bitcast.9, f32[2,256]{1,0:T(2,128)} %bitcast.10, f32[2]{0:T(128)} %sinks.1, ...), custom_call_target="tpu_custom_call" | custom-call | tf_op jit(solution)/shard_map/layer/pallas_call | solution.py:750
  154.9 1.6 %copy.18 = bf16[256,256]{1,0:T(8,128)(2,1)} copy(bf16[256,256]{1,0:T(8,128)(2,1)} %layer.1) | data formatting | bytes 262144
